TPU v7x, 256 devices: a whole 4x4x8 slice. The times are simulated.
256 devices in a mesh: ep: 128 (over z, y, x), tp: 2 (over core).
Axes of the slice: x: 4, y: 4, z: 8, core: 2. Of those that a mesh axis runs over, the one named last changes fastest.
Arguments:
- tokens: bfloat16 [2048, 2048], P('ep'), may hold values from -6 to 6
- lengths: int32 [2048], P('ep'), may hold values from 1024 to 8191
- prior_state: float32 [2048, 16, 64, 64], P('ep', 'tp'), may hold values from -2 to 2
- mix_gain: float32 [2048], replicated, may hold values from 0.1 to 1.9
- post_gain: float32 [2048], replicated, may hold values from 0.1 to 1.9
- ffn_gain: float32 [2048], replicated, may hold values from 0.1 to 1.9
- out_gain: float32 [2048], replicated, may hold values from 0.1 to 1.9
- query_weight: bfloat16 [2048, 1024], P('ep', 'tp'), may hold values from -0.125 to 0.125
- key_weight: bfloat16 [2048, 1024], P('ep', 'tp'), may hold values from -0.125 to 0.125
- value_weight: bfloat16 [2048, 1024], P('ep', 'tp'), may hold values from -0.125 to 0.125
- gate_weight: bfloat16 [2048, 1024], P('ep', 'tp'), may hold values from -0.125 to 0.125
- out_weight: bfloat16 [1024, 2048], P('tp', 'ep'), may hold values from -0.1875 to 0.1875
- routes: int32 [2048, 6], P('ep'), may hold values from 0 to 127, all different within a row; in each aligned block of 16 rows (0 to 15, 16 to 31, ...) at most 2 rows name the same one
- route_gates: float32 [2048, 6], P('ep'), may hold values from 0.1 to 0.9
- expert_gate: bfloat16 [128, 2048, 512], P('ep', None, 'tp'), may hold values from -0.125 to 0.125
- expert_up: bfloat16 [128, 2048, 512], P('ep', None, 'tp'), may hold values from -0.125 to 0.125
- expert_down: bfloat16 [128, 512, 2048], P('ep', 'tp'), may hold values from -0.25 to 0.25
- shared_gate: bfloat16 [2048, 512], P(None, 'tp'), may hold values from -0.125 to 0.125
- shared_up: bfloat16 [2048, 512], P(None, 'tp'), may hold values from -0.125 to 0.125
- shared_down: bfloat16 [512, 2048], P('tp'), may hold values from -0.25 to 0.25
Outputs:
- result: bfloat16 [2048, 2048], P('ep')
- new_state: float32 [2048, 16, 64, 64], P('ep', 'tp')
Inputs may be any that keep to these rules, and one draw needn't show every extreme that they name: `routes`: each row names 6 different experts. In the rows of one device (aligned blocks of 16 rows) no expert is named more than 2 times, and in every draw some expert is named exactly 2 times in some block.
All inputs are finite; a program needn't handle non-finite values.
Results may differ from a plain program's by a relative error of at most 0.02.
Values may be sent and summed in bfloat16 or wider, within the bound.
A program may use at most 128 MiB of HBM per device.

v0:
```python
import jax
import jax.numpy as jnp
from jax import lax
from jax.sharding import Mesh
from jax.sharding import PartitionSpec as P

HEAD = 64
HEADS = 16
EP = ("ep_0", "ep_1", "ep_2")


EPS = 1e-06
THETA = 10000.0


def sent_together(arrays, axis, dim, along):
    widths = [a.shape[along] for a in arrays]
    both = jnp.concatenate(arrays, axis=along)
    out = lax.all_gather(both, axis, axis=dim, tiled=True)
    return tuple(jnp.split(out, [sum(widths[:k]) for k in range(1, len(widths))], axis=along))


def gathered_by_axis(value, axes, dim):
    for axis in reversed(axes):
        value = lax.all_gather(value, axis, axis=dim, tiled=True)
    return value


def sent_to_all(value, axis):
    copies = jnp.broadcast_to(value, (lax.axis_size(axis), *value.shape))
    return lax.all_to_all(copies, axis, split_axis=0, concat_axis=0, tiled=True)


def of_everyone(value, axis):
    return sent_to_all(value, axis).astype(jnp.float32).sum(axis=0)


def split_up(value, dim, count):
    before, after = (value.shape[:dim], value.shape[dim + 1 :])
    return jnp.moveaxis(value.reshape(*before, count, -1, *after), dim, 0)


def summed_on_arrival(value, axis, dim):
    count = lax.axis_size(axis)
    blocks = lax.all_to_all(split_up(value, dim, count), axis, 0, 0, tiled=True)
    return jnp.sum(blocks.astype(jnp.float32), axis=0)


def gathered_total(value, axis):
    blocks = lax.all_gather(value, axis)
    return blocks.sum(axis=0)


def in_order(blocks, dim):
    shape = list(blocks.shape[1:])
    shape[dim] *= blocks.shape[0]
    return jnp.moveaxis(blocks, 0, dim).reshape(shape)


def gathered_copies(value, axis, dim):
    blocks = sent_to_all(value, axis)
    return in_order(blocks, dim)


def rounded(values):
    return lax.optimization_barrier(values.astype(jnp.bfloat16)).astype(jnp.float32)


def scaled_rows(values, gain_row):
    widened = values.astype(jnp.float32)
    return widened * lax.rsqrt(jnp.mean(widened * widened, axis=-1, keepdims=True) + EPS) * gain_row


def rotate(vectors, lengths):
    half_dim = vectors.shape[-1] // 2
    frequency = THETA ** (-jnp.arange(half_dim, dtype=jnp.float32) / half_dim)
    angles = lengths.astype(jnp.float32)[:, None] * frequency[None, :]
    cosine = jnp.cos(angles)[:, None, :]
    sine_part = jnp.sin(angles)[:, None, :]
    leading = vectors[..., :half_dim]
    trailing = vectors[..., half_dim:]
    return jnp.concatenate(
        [leading * cosine - trailing * sine_part, trailing * cosine + leading * sine_part], axis=-1
    )


def decay_table(head_count):
    head_order = jnp.arange(head_count, dtype=jnp.float32)
    return 1.0 - jnp.exp2(-5.0 - 7.0 * head_order / (head_count - 1))


def retain(queries, keys_new, values, out_gate, prior_state, lengths, decays):
    seq_count = queries.shape[0]
    head_count = decays.shape[0]
    layout = (seq_count, head_count, HEAD)
    rot_query = rotate(queries.astype(jnp.float32).reshape(layout), lengths)
    rot_key = rotate(keys_new.astype(jnp.float32).reshape(layout), lengths) * HEAD ** (-0.5)
    wide_values = values.astype(jnp.float32).reshape(layout)
    from_state = jnp.einsum("shd,shde->she", rot_query, prior_state)
    self_term = jnp.sum(rot_query * rot_key, axis=-1, keepdims=True)
    read_out = decays[None, :, None] * from_state + self_term * wide_values
    new_state = (
        decays[None, :, None, None] * prior_state
        + rot_key[..., :, None] * wide_values[..., None, :]
    )
    normed = read_out * lax.rsqrt(jnp.mean(read_out * read_out, axis=-1, keepdims=True) + EPS)
    gated_rows = normed.reshape(seq_count, head_count * HEAD) * jax.nn.silu(
        out_gate.astype(jnp.float32)
    )
    return (gated_rows.astype(jnp.bfloat16), new_state)


def on_device(
    tokens,
    lengths,
    prior_state,
    mix_gain,
    post_gain,
    ffn_gain,
    out_gain,
    query_weight,
    key_weight,
    value_weight,
    gate_weight,
    out_weight,
    routes,
    route_gates,
    expert_gate,
    expert_up,
    expert_down,
    shared_gate,
    shared_up,
    shared_down,
):
    seq_here = tokens.shape[0]
    model_width = tokens.shape[1]
    local_cols = query_weight.shape[1]
    normed = scaled_rows(tokens, mix_gain).astype(jnp.bfloat16)
    pieces = sent_together((query_weight, key_weight, value_weight, gate_weight), EP, 0, 1)
    projected = tuple(
        (jnp.dot(normed, portion, preferred_element_type=jnp.float32) for portion in pieces)
    )
    queries, keys_new, values, out_gate = tuple(
        (member.astype(jnp.bfloat16) for member in projected)
    )
    heads_here = local_cols // HEAD
    decays = lax.dynamic_slice_in_dim(
        decay_table(HEADS), lax.axis_index("tp") * heads_here, heads_here, 0
    )
    retained, new_state = retain(queries, keys_new, values, out_gate, prior_state, lengths, decays)
    partial_mix = jnp.dot(
        retained, gathered_by_axis(out_weight, EP, 1), preferred_element_type=jnp.float32
    )
    mixed_sum = rounded(
        of_everyone(rounded(partial_mix).astype(jnp.bfloat16), "tp").astype(jnp.float32)
    )
    middle = rounded(tokens.astype(jnp.float32) + scaled_rows(mixed_sum, post_gain))
    moe_in = scaled_rows(middle, ffn_gain).astype(jnp.bfloat16)
    experts_all = lax.axis_size(EP)
    topk_here = routes.shape[1]
    capacity = seq_here * topk_here // experts_all + 2
    slot_count = experts_all * capacity
    flat_routes = routes.reshape(-1)
    onehot = (flat_routes[:, None] == jnp.arange(experts_all, dtype=jnp.int32)[None, :]).astype(
        jnp.int32
    )
    earlier = jnp.cumsum(onehot, axis=0) - onehot
    ranks = jnp.sum(earlier * onehot, axis=1)
    slot_ids = flat_routes * capacity + ranks
    placing = (jnp.arange(slot_count, dtype=jnp.int32)[:, None] == slot_ids[None, :]).reshape(
        slot_count, seq_here, topk_here
    )
    dispatch_rows = jnp.any(placing, axis=2).astype(jnp.bfloat16)
    combine = jnp.sum(
        jnp.where(placing, route_gates[None, :, :], jnp.zeros((), jnp.float32)), axis=2
    ).T
    outgoing = jnp.dot(dispatch_rows, moe_in, preferred_element_type=jnp.float32).astype(
        jnp.bfloat16
    )
    outgoing = outgoing.reshape(experts_all, capacity, model_width)
    gate_local = expert_gate[0]
    up_local = expert_up[0]
    down_local = expert_down[0]
    arrived = lax.all_to_all(outgoing, EP, split_axis=0, concat_axis=0, tiled=True)
    sources = arrived.shape[0]
    held_slots = arrived.shape[1]
    flat_in = arrived.reshape(sources * held_slots, model_width)
    hidden = (
        jax.nn.silu(jnp.dot(flat_in, gate_local, preferred_element_type=jnp.float32))
        * jnp.dot(flat_in, up_local, preferred_element_type=jnp.float32)
    ).astype(jnp.bfloat16)
    partial_out = rounded(jnp.dot(hidden, down_local, preferred_element_type=jnp.float32))
    expert_sum = summed_on_arrival(partial_out.astype(jnp.bfloat16), "tp", 1).astype(jnp.bfloat16)
    returned = lax.all_to_all(
        expert_sum.reshape(sources, held_slots, -1), EP, split_axis=0, concat_axis=0, tiled=True
    )
    back_rows = returned.reshape(slot_count, -1).astype(jnp.float32)
    routed = jnp.dot(combine, back_rows)
    shared_hidden = (
        jax.nn.silu(jnp.dot(moe_in, shared_gate, preferred_element_type=jnp.float32))
        * jnp.dot(moe_in, shared_up, preferred_element_type=jnp.float32)
    ).astype(jnp.bfloat16)
    shared_part = rounded(jnp.dot(shared_hidden, shared_down, preferred_element_type=jnp.float32))
    shared_out = summed_on_arrival(shared_part.astype(jnp.bfloat16), "tp", 1).astype(jnp.bfloat16)
    mixture = shared_out.astype(jnp.float32) + routed
    squares = gathered_total(jnp.sum(mixture * mixture, axis=1, keepdims=True), "tp")
    half_cols = mixture.shape[1]
    offset = lax.axis_index("tp") * half_cols
    gain_part = lax.dynamic_slice_in_dim(out_gain, offset, half_cols, 0)
    middle_part = lax.dynamic_slice_in_dim(middle, offset, half_cols, 1)
    scale_rows = lax.rsqrt(squares / model_width + EPS)
    half_result = (middle_part + mixture * scale_rows * gain_part).astype(jnp.bfloat16)
    result = gathered_copies(half_result, "tp", 1)
    return (result, new_state)


def solution(mesh):
    finer = Mesh(mesh.devices.reshape(8, 4, 4, mesh.shape["tp"]), ("ep_0", "ep_1", "ep_2", "tp"))
    in_specs = (
        P(EP, None),
        P(EP),
        P(EP, "tp", None, None),
        P(),
        P(),
        P(),
        P(),
        P(EP, "tp"),
        P(EP, "tp"),
        P(EP, "tp"),
        P(EP, "tp"),
        P("tp", EP),
        P(EP, None),
        P(EP, None),
        P(EP, None, "tp"),
        P(EP, None, "tp"),
        P(EP, "tp", None),
        P(None, "tp"),
        P(None, "tp"),
        P("tp", None),
    )
    out_specs = (P(EP, None), P(EP, "tp", None, None))
    return jax.shard_map(
        on_device, mesh=finer, in_specs=in_specs, out_specs=out_specs, check_vma=False
    )
```

profile of v0, /device:TPU:1, one launch (start us, length us, event | category | flops | bytes accessed | tf_op | source)
XLA Modules:
  0.0 289.7 jit_solution(9632476741348007114)
XLA Ops:
  7.3 1.5 pad_maximum_fusion
  8.8 10.4 %all_gather.16 = bf16[512,64]{0,1:T(8,128)(2,1)S(1)} all-gather(bf16[512,16]{0,1:T(8,128)(2,1)} %param.31), channel_id=1, replica_groups=mesh['ep_0'=8,'ep_1'=4,'ep_2'=4,'tp'=2] {'ep_2'}, dimensions={1}, use_global_device_ids=true | all-gather | bytes 81920 | tf_op jit(solution)/shard_map/all_gather | solution.py:25
  19.2 10.6 %all_gather.17 = bf16[512,256]{0,1:T(8,128)(2,1)} all-gather(bf16[512,64]{0,1:T(8,128)(2,1)S(1)} %all_gather.16), channel_id=1, replica_groups=mesh['ep_0'=8,'ep_1'=4,'ep_2'=4,'tp'=2] {'ep_1'}, dimensions={1}, use_global_device_ids=true | all-gather | bytes 327680 | tf_op jit(solution)/shard_map/all_gather | solution.py:25
  29.8 0.7 convert_element_type.88
  30.5 0.8 copy.46
  32.0 0.7 multiply_add_fusion.3
  32.8 1.0 fusion.49
  33.9 102.7 %all-gather.4.cloned.1.call-done = bf16[2048,2048]{1,0:T(8,128)(2,1)} async-done(((bf16[16,2048]{1,0:T(8,128)(2,1)}), bf16[2048,2048]{1,0:T(8,128)(2,1)}) %all-gather.4.cloned.1.call-update) | async-done | bytes 8388624 | tf_op jit(solution)/shard_map/all_gather | solution.py:19
  136.6 2.1 fusion.15
  138.7 2.1 fusion.21
  140.9 2.0 fusion.27
  143.2 2.8 fusion.77
  146.5 29.0 %all-gather.6.cloned.1.call-done = bf16[512,2048]{0,1:T(8,128)(2,1)} async-done(((bf16[512,256]{0,1:T(8,128)(2,1)}), bf16[512,2048]{0,1:T(8,128)(2,1)}) %all-gather.6.cloned.1.call-update) | async-done | bytes 2097168 | tf_op jit(solution)/shard_map/all_gather | solution.py:25
  175.5 3.3 %convolution_convert_fusion.3 = bf16[16,2048]{1,0:T(8,128)(2,1)S(1)} fusion(bf16[512,2048]{0,1:T(8,128)(2,1)} %all-gather.6.cloned.1.call-done, f32[16,512]{1,0:T(8,128)S(1)} %reshape.187, bf16[2048,2048]{1,0:T(8,128)(2,1)} %all-gather.4.cloned.1.call-done, bf16[16,2048]{1,0:T(8,128)(2,1)S(1)} %copy-done.2, f32[2048]{0:T(1024)S(1)} %copy-done.4, ...), kind=kOutput, calls=%fused_computation.5 | convolution fusion | flops 67338240 | bytes 4366400 | tf_op jit(solution)/shard_map/dot_general | solution.py:151
  178.8 8.5 %all_to_all.30 = bf16[2,16,2048]{2,1,0:T(8,128)(2,1)S(1)} all-to-all(bf16[2,16,2048]{2,1,0:T(8,128)(2,1)S(1)} %broadcast_in_dim.12), channel_id=1, replica_groups=mesh['ep_0'=8,'ep_1'=4,'ep_2'=4,'tp'=2] {'tp'}, dimensions={0} | all-to-all | bytes 262144 | tf_op jit(solution)/shard_map/all_to_all | solution.py:31
  188.1 1.5 reshape.189
  189.6 11.1 %all-to-all-start.2 = ((bf16[128,2,2048]{2,1,0:T(2,128)(2,1)}), bf16[128,2,2048]{2,1,0:T(2,128)(2,1)S(1)}, u32[]{:S(2)}, u32[]{:S(2)}) async-start(bf16[128,2,2048]{2,1,0:T(2,128)(2,1)} %reshape.189), calls=%async_computation.2 | async-start | bytes 2097152 | tf_op jit(solution)/shard_map/all_to_all | solution.py:184
  200.7 1.5 fusion.71
  202.3 2.0 convolution_convert_fusion.2
  204.3 0.7 copy.58
  204.9 25.0 %all-to-all-done.2 = bf16[128,2,2048]{2,1,0:T(2,128)(2,1)S(1)} async-done(((bf16[128,2,2048]{2,1,0:T(2,128)(2,1)}), bf16[128,2,2048]{2,1,0:T(2,128)(2,1)S(1)}, u32[]{:S(2)}, u32[]{:S(2)}) %all-to-all-start.2) | async-done | bytes 1048608 | tf_op jit(solution)/shard_map/all_to_all | solution.py:184
  230.3 2.4 fusion.40
  232.7 2.5 convolution_convert_fusion.1
  235.3 7.3 %all_to_all.31 = bf16[2,256,1024]{2,1,0:T(8,128)(2,1)S(1)} all-to-all(bf16[2,256,1024]{2,1,0:T(8,128)(2,1)S(1)} %bitcast.44), channel_id=1, replica_groups=mesh['ep_0'=8,'ep_1'=4,'ep_2'=4,'tp'=2] {'tp'}, dimensions={0} | all-to-all | bytes 2097152 | tf_op jit(solution)/shard_map/all_to_all | solution.py:45
  242.6 3.7 %all-to-all-start.1 = ((bf16[2,16,1024]{2,1,0:T(8,128)(2,1)}), bf16[2,16,1024]{2,1,0:T(8,128)(2,1)S(1)}, u32[]{:S(2)}, u32[]{:S(2)}) async-start(bf16[2,16,1024]{2,1,0:T(8,128)(2,1)} %bitcast.43), calls=%async_computation.1 | async-start | bytes 131072 | tf_op jit(solution)/shard_map/all_to_all | solution.py:45
  246.5 1.0 reshape.192
  247.5 6.2 %all-to-all-start.4 = ((bf16[128,2,1024]{2,1,0:T(2,128)(2,1)}), bf16[128,2,1024]{2,1,0:T(2,128)(2,1)S(1)}, u32[]{:S(2)}, u32[]{:S(2)}) async-start(bf16[128,2,1024]{2,1,0:T(2,128)(2,1)} %reshape.192), calls=%async_computation.4 | async-start | bytes 1048576 | tf_op jit(solution)/shard_map/all_to_all | solution.py:194
  255.1 4.3 %multiply_add_fusion = f32[16,8,64,64]{3,2,1,0:T(8,128)} fusion(f32[16,8,64,64]{3,2,1,0:T(8,128)} %param.22, f32[16,8,64]{2,1,0:T(8,128)S(1)} %reshape.200, f32[16,8,64]{2,1,0:T(8,128)S(1)} %get-tuple-element.15, f32[8]{0:T(128)S(1)} %dynamic_slice.9), kind=kLoop, calls=%fused_computation.1 | loop fusion | flops 1572864 | bytes 4259872 | tf_op jit(solution)/shard_map/add | solution.py:103
  259.4 13.7 %all-to-all-done.4 = bf16[128,2,1024]{2,1,0:T(2,128)(2,1)S(1)} async-done(((bf16[128,2,1024]{2,1,0:T(2,128)(2,1)}), bf16[128,2,1024]{2,1,0:T(2,128)(2,1)S(1)}, u32[]{:S(2)}, u32[]{:S(2)}) %all-to-all-start.4) | async-done | bytes 524320 | tf_op jit(solution)/shard_map/all_to_all | solution.py:194
  273.8 4.4 %all-reduce = f32[32]{0:T(128)S(1)} all-reduce(f32[32]{0:T(128)S(1)} %dynamic-update-slice), channel_id=2, replica_groups=mesh['ep_0'=8,'ep_1'=4,'ep_2'=4,'tp'=2] {'tp'}, use_global_device_ids=true, to_apply=%add | all-reduce | flops 32 | bytes 256
  278.4 3.8 %all_to_all.32 = bf16[2,16,1024]{2,1,0:T(8,128)(2,1)S(1)} all-to-all(bf16[2,16,1024]{2,1,0:T(8,128)(2,1)S(1)} %broadcast_in_dim.15), channel_id=1, replica_groups=mesh['ep_0'=8,'ep_1'=4,'ep_2'=4,'tp'=2] {'tp'}, dimensions={0} | all-to-all | bytes 131072 | tf_op jit(solution)/shard_map/all_to_all | solution.py:31
  282.2 0.6 copy.54
  (68 shorter events, 5.3 us)
Async XLA Ops:
  7.2 225.5 %copy-start = (bf16[1,256,2048]{2,1,0:T(8,128)(2,1)S(1)}, bf16[1,256,2048]{2,1,0:T(8,128)(2,1)}, u32[]{:S(2)}) copy-start(bf16[1,256,2048]{2,1,0:T(8,128)(2,1)} %param.36) | copy-start | bytes 3145732
  7.2 133.7 %copy-start.2 = (bf16[16,2048]{1,0:T(8,128)(2,1)S(1)}, bf16[16,2048]{1,0:T(8,128)(2,1)}, u32[]{:S(2)}) copy-start(bf16[16,2048]{1,0:T(8,128)(2,1)} %param.20) | copy-start | bytes 196612
  7.2 133.7 %copy-start.4 = (f32[2048]{0:T(1024)S(1)}, f32[2048]{0:T(1024)}, u32[]{:S(2)}) copy-start(f32[2048]{0:T(1024)} %param.23) | copy-start | bytes 24580
  7.2 129.4 %all-gather.4.cloned.1.call-start = ((), (), s32[]{:S(2)}) async-start(), calls=%async_computation.6 | async-start | bytes 8454144 | tf_op jit(solution)/shard_map/all_gather | solution.py:19
  8.8 166.7 %all-gather.6.cloned.1.call-start = ((), (), s32[]{:S(2)}) async-start(), calls=%async_computation.7 | async-start | bytes 2359296 | tf_op jit(solution)/shard_map/all_gather | solution.py:25
  143.2 44.2 %copy-start.5 = (f32[2048]{0:T(1024)S(1)}, f32[2048]{0:T(1024)}, u32[]{:S(2)}) copy-start(f32[2048]{0:T(1024)} %param.24) | copy-start | bytes 24580
  143.2 44.4 %copy-start.3 = (f32[2048]{0:T(1024)S(1)}, f32[2048]{0:T(1024)}, u32[]{:S(2)}) copy-start(f32[2048]{0:T(1024)} %param.25) | copy-start | bytes 24580
  178.7 23.5 %copy-start.1 = (bf16[256,2048]{1,0:T(8,128)(2,1)S(1)}, bf16[256,2048]{1,0:T(8,128)(2,1)}, u32[]{:S(2)}) copy-start(bf16[256,2048]{1,0:T(8,128)(2,1)} %param.39) | copy-start | bytes 3145732
  189.6 40.2 %all-to-all-start.2 = ((bf16[128,2,2048]{2,1,0:T(2,128)(2,1)}), bf16[128,2,2048]{2,1,0:T(2,128)(2,1)S(1)}, u32[]{:S(2)}, u32[]{:S(2)}) async-start(bf16[128,2,2048]{2,1,0:T(2,128)(2,1)} %reshape.189), calls=%async_computation.2 | async-start | bytes 2097152 | tf_op jit(solution)/shard_map/all_to_all | solution.py:184
  235.2 18.5 %copy-start.7 = (u32[256]{0:T(256)S(1)}, u32[256]{0:T(256)}, u32[]{:S(2)}) copy-start(u32[256]{0:T(256)} %constant.79) | copy-start | bytes 3076
  235.3 19.7 %copy-start.6 = (f32[16,6]{0,1:T(8,128)S(1)}, f32[16,6]{0,1:T(8,128)}, u32[]{:S(2)}) copy-start(f32[16,6]{0,1:T(8,128)} %param.33) | copy-start | bytes 1156
  242.6 4.9 %all-to-all-start.1 = ((bf16[2,16,1024]{2,1,0:T(8,128)(2,1)}), bf16[2,16,1024]{2,1,0:T(8,128)(2,1)S(1)}, u32[]{:S(2)}, u32[]{:S(2)}) async-start(bf16[2,16,1024]{2,1,0:T(8,128)(2,1)} %bitcast.43), calls=%async_computation.1 | async-start | bytes 131072 | tf_op jit(solution)/shard_map/all_to_all | solution.py:45
  247.5 25.6 %all-to-all-start.4 = ((bf16[128,2,1024]{2,1,0:T(2,128)(2,1)}), bf16[128,2,1024]{2,1,0:T(2,128)(2,1)S(1)}, u32[]{:S(2)}, u32[]{:S(2)}) async-start(bf16[128,2,1024]{2,1,0:T(2,128)(2,1)} %reshape.192), calls=%async_computation.4 | async-start | bytes 1048576 | tf_op jit(solution)/shard_map/all_to_all | solution.py:194
  255.1 23.2 %dynamic-slice-start = ((f32[2048]{0:T(1024)}, s32[]{:T(128)}), f32[1024]{0:T(1024)S(1)}, s32[]{:S(2)}) async-start(f32[2048]{0:T(1024)} %param.26, s32[]{:T(128)} %select_n.12), calls=%async_computation.8 | async-start | bytes 8704 | tf_op jit(solution)/shard_map/dynamic_slice | solution.py:209
Sparse Core Ops, SparseCore 0:
  12.2 124.3 all-gather.3
  138.4 37.0 all-gather.5
where the time goes:
time: 291 us; the launch traced here: 290 us
  waiting for transfers between devices  170 us (58%)
  blocking collectives  44.9 us (15%)
  matrix products  21.4 us (7%)
  starting transfers between devices  21 us (7%)
  between operations  15 us (5%)
  other arithmetic  10.1 us (3%)
  local copies, waits for them, and re-layouts  6.89 us (2%)
    all_gather x1, waiting for transfers between devices, sent_together(): out = lax.all_gather(both, axis, axis=dim, tiled=True)  103 us
    all_gather x1, waiting for transfers between devices, gathered_by_axis(): value = lax.all_gather(value, axis, axis=dim, tiled=True)  29 us
    all_to_all x1, waiting for transfers between devices, on_device(): lax.all_to_all(outgoing, EP, split_axis=0, concat_axis=0, tiled=True)  25 us
    all_gather x2, blocking collectives, gathered_by_axis(): value = lax.all_gather(value, axis, axis=dim, tiled=True)  21 us
    all_to_all x1, waiting for transfers between devices, on_device(): lax.all_to_all(expert_sum.reshape(sources, held_slots, -1), EP, split_axi...  13.7 us
    all_to_all x2, blocking collectives, sent_to_all(): return lax.all_to_all(copies, axis, split_axis=0, concat_axis=0, tiled=True)  12.3 us
    all_to_all x1, starting transfers between devices, on_device(): lax.all_to_all(outgoing, EP, split_axis=0, concat_axis=0, tiled=True)  11.1 us
    all_to_all x1, blocking collectives, summed_on_arrival(): blocks = lax.all_to_all(split_up(value, dim, count), axis, 0, 0, tiled=True)  7.25 us
  transfers between devices with their start and end apart: 5, of which 4 were waited for; matrix products, arithmetic and copies ran while one was open for 8% of the time, Pallas kernels for 0%

commit v1 on v0

--- a/solution.py
+++ b/solution.py
@@ -1,6 +1,8 @@
 import jax
 import jax.numpy as jnp
 from jax import lax
+from jax.experimental import pallas as pl
+from jax.experimental.pallas import tpu as pltpu
 from jax.sharding import Mesh
 from jax.sharding import PartitionSpec as P
 
@@ -108,6 +110,224 @@
         out_gate.astype(jnp.float32)
     )
     return (gated_rows.astype(jnp.bfloat16), new_state)
+
+
+MESH = pl.DeviceIdType.MESH
+NZ, NY, NX, NG = 8, 4, 4, 16
+BF16 = jnp.bfloat16
+
+
+def place():
+    z, y, x, c = (lax.axis_index(name) for name in ("ep_0", "ep_1", "ep_2", "tp"))
+    return z, y * NX + x, c
+
+
+def device(z, g, c):
+    return (z, g // NX, g % NX, c)
+
+
+def remote(src, dst, send_sem, recv_sem, target):
+    return pltpu.make_async_remote_copy(
+        src_ref=src,
+        dst_ref=dst,
+        send_sem=send_sem,
+        recv_sem=recv_sem,
+        device_id=target,
+        device_id_type=MESH,
+    )
+
+
+def each(low, high, body):
+    def step(i, carry):
+        body(i)
+        return carry
+
+    lax.fori_loop(low, high, step, 0)
+
+
+def greet(z, g, c):
+    barrier = pltpu.get_barrier_semaphore()
+
+    def in_plane(i):
+        pl.semaphore_signal(
+            barrier, inc=1, device_id=device(z, (g + i) % NG, c), device_id_type=MESH
+        )
+
+    def in_column(j):
+        other = (z * 2 + c + j) % (2 * NZ)
+        pl.semaphore_signal(
+            barrier, inc=1, device_id=device(other // 2, g, other % 2), device_id_type=MESH
+        )
+
+    each(1, NG, in_plane)
+    each(1, 2 * NZ, in_column)
+    return barrier
+
+
+def project_kernel(
+    tokens_ref, gain_ref, wsrc_ref, wot_ref, out_ref, wo_ref,
+    tbuf, abuf, wbuf, zbuf, xsend, xbuf, osend,
+    t_s, t_r, a_s, a_r, b_s, b_r, c_s, c_r, d_s, d_r, x_s, x_r, o_s, o_r, l_s,
+):
+    z, g, c = place()
+    barrier = greet(z, g, c)
+    half = tbuf.shape[-1]
+    wide = tokens_ref[...].astype(jnp.float32)
+    scale = lax.rsqrt(jnp.mean(wide * wide, axis=-1, keepdims=True) + EPS)
+    cols = pl.ds(pl.multiple_of(c * half, 128), half)
+    part = tokens_ref[:, cols].astype(jnp.float32)
+    tbuf[pl.ds(g, 1)] = (part * scale * gain_ref[:, cols]).astype(BF16)[None]
+    pl.semaphore_wait(barrier, NG - 1 + 2 * NZ - 1)
+
+    def plane_copy(src, dst, send, recv, i):
+        other = (g + i) % NG
+        return remote(src(other), dst(g), send.at[other], recv.at[g], device(z, other, c))
+
+    def plane_recv(src, dst, send, recv, i):
+        other = (g + i) % NG
+        return remote(src(other), dst(other), send.at[other], recv.at[other], device(z, other, c))
+
+    def a_args():
+        return (lambda k: wsrc_ref.at[k], lambda k: abuf.at[k], a_s, a_r)
+
+    def t_args():
+        return (lambda k: tbuf.at[g], lambda k: tbuf.at[k], t_s, t_r)
+
+    def o_args():
+        return (lambda k: osend.at[k], lambda k: out_ref.at[k], o_s, o_r)
+
+    each(1, NG, lambda i: plane_copy(*a_args(), i).start())
+    own_a = pltpu.make_async_copy(wsrc_ref.at[g], abuf.at[g], l_s.at[0])
+    own_a.start()
+
+    def c_copy(j, recv):
+        other = (z + j) % NZ
+        slot = other if recv else z
+        return remote(wot_ref, zbuf.at[slot], c_s.at[other], c_r.at[slot], device(other, g, c))
+
+    each(1, NG, lambda i: plane_copy(*t_args(), i).start())
+    each(1, NZ, lambda j: c_copy(j, False).start())
+    own_z = pltpu.make_async_copy(wot_ref, zbuf.at[z], l_s.at[1])
+    own_z.start()
+
+    each(1, NG, lambda i: plane_recv(*a_args(), i).wait_recv())
+    own_a.wait()
+    b_core = z // (NZ // 2)
+
+    def b_copy(j):
+        other = (z + j) % NZ
+        return remote(
+            abuf, wbuf.at[c, z % 4], b_s.at[j], b_r.at[c, z % 4], device(other, g, b_core)
+        )
+
+    each(1, NZ, lambda j: b_copy(j).start())
+
+    @pl.when(b_core == c)
+    def _():
+        pltpu.make_async_copy(abuf, wbuf.at[c, z % 4], b_r.at[c, z % 4]).start()
+
+    @pl.when(b_core != c)
+    def _():
+        b_copy(0).start()
+
+    each(1, NZ, lambda j: c_copy(j, True).wait_recv())
+    own_z.wait()
+    to_half = g // (NG // 2)
+
+    def d_copy(k):
+        other = 2 * k + to_half
+        return other, remote(
+            zbuf.at[k], wo_ref.at[g % 8], d_s.at[k], d_r.at[g % 8], device(z, other, c)
+        )
+
+    def d_start(k):
+        other, copy = d_copy(k)
+
+        @pl.when(other == g)
+        def _():
+            pltpu.make_async_copy(zbuf.at[k], wo_ref.at[g % 8], d_r.at[g % 8]).start()
+
+        @pl.when(other != g)
+        def _():
+            copy.start()
+
+    each(0, NZ, d_start)
+
+    each(1, NG, lambda i: plane_recv(*t_args(), i).wait_recv())
+
+    def b_wait(j):
+        pltpu.make_async_copy(abuf, wbuf.at[j // 4, j % 4], b_r.at[j // 4, j % 4]).wait()
+
+    each(0, NZ, b_wait)
+    rows = NG * tbuf.shape[1]
+    normed = tbuf[...].reshape(rows, half)
+
+    def weights(k):
+        return wbuf[pl.ds(k, 1)].reshape(half, 128)
+
+    xsend[...] = jnp.dot(normed, weights(1 - c), preferred_element_type=jnp.float32)
+    swap = remote(xsend, xbuf, x_s, x_r, device(z, g, 1 - c))
+    swap.start()
+    mine = jnp.dot(normed, weights(c), preferred_element_type=jnp.float32)
+    swap.wait_recv()
+    osend[...] = (mine + xbuf[...]).astype(BF16).reshape(osend.shape)
+    each(1, NG, lambda i: plane_copy(*o_args(), i).start())
+    own_o = pltpu.make_async_copy(osend.at[g], out_ref.at[g], l_s.at[2])
+    own_o.start()
+
+    def d_wait(k):
+        pltpu.make_async_copy(zbuf.at[k], wo_ref.at[k], d_r.at[k]).wait()
+
+    each(0, NZ, d_wait)
+    each(1, NG, lambda i: plane_recv(*o_args(), i).wait_recv())
+    own_o.wait()
+    for args in (a_args(), t_args(), o_args()):
+        each(1, NG, lambda i, args=args: plane_copy(*args, i).wait_send())
+    each(1, NZ, lambda j: c_copy(j, False).wait_send())
+    each(1, NZ, lambda j: b_copy(j).wait_send())
+
+    @pl.when(b_core != c)
+    def _():
+        b_copy(0).wait_send()
+
+    def d_sent(k):
+        other, copy = d_copy(k)
+
+        @pl.when(other != g)
+        def _():
+            copy.wait_send()
+
+    each(0, NZ, d_sent)
+    swap.wait_send()
+
+
+def project(tokens, mix_gain, weights, out_weight):
+    seq, width = tokens.shape
+    wsrc = jnp.concatenate(weights, axis=1).reshape(seq, NG, 128).transpose(1, 0, 2)
+    dma = pltpu.SemaphoreType.DMA
+    return pl.pallas_call(
+        project_kernel,
+        out_shape=(
+            jax.ShapeDtypeStruct((NG, seq, 128), BF16),
+            jax.ShapeDtypeStruct((8, 16, 512), BF16),
+        ),
+        in_specs=[pl.BlockSpec(memory_space=pltpu.VMEM)] * 4,
+        out_specs=(pl.BlockSpec(memory_space=pltpu.VMEM),) * 2,
+        scratch_shapes=[
+            pltpu.VMEM((NG, seq, width // 2), BF16),
+            pltpu.VMEM((NG, 16, 128), BF16),
+            pltpu.VMEM((2, 4, NG, 16, 128), BF16),
+            pltpu.VMEM((8, 16, 512), BF16),
+            pltpu.VMEM((NG * seq, 128), jnp.float32),
+            pltpu.VMEM((NG * seq, 128), jnp.float32),
+            pltpu.VMEM((NG, seq, 128), BF16),
+            dma((NG,)), dma((NG,)), dma((NG,)), dma((NG,)),
+            dma((NZ,)), dma((2, 4)), dma((NZ,)), dma((NZ,)), dma((NZ,)), dma((NZ,)),
+            dma, dma, dma((NG,)), dma((NG,)), dma((3,)),
+        ],
+        compiler_params=pltpu.CompilerParams(collective_id=0, has_side_effects=True),
+        name="project",
+    )(tokens, mix_gain[None], wsrc, out_weight.T)
 
 
 def on_device(
@@ -135,13 +355,11 @@
     seq_here = tokens.shape[0]
     model_width = tokens.shape[1]
     local_cols = query_weight.shape[1]
-    normed = scaled_rows(tokens, mix_gain).astype(jnp.bfloat16)
-    pieces = sent_together((query_weight, key_weight, value_weight, gate_weight), EP, 0, 1)
-    projected = tuple(
-        (jnp.dot(normed, portion, preferred_element_type=jnp.float32) for portion in pieces)
-    )
-    queries, keys_new, values, out_gate = tuple(
-        (member.astype(jnp.bfloat16) for member in projected)
+    blocks, wo_blocks = project(
+        tokens, mix_gain, (query_weight, key_weight, value_weight, gate_weight), out_weight
+    )
+    queries, keys_new, values, out_gate = (
+        blocks[4 * k : 4 * k + 4].transpose(1, 0, 2).reshape(seq_here, local_cols) for k in range(4)
     )
     heads_here = local_cols // HEAD
     decays = lax.dynamic_slice_in_dim(

time: 291 us -> 196 us (0.67)
  waiting for transfers between devices: 170 us -> 38.7 us
  Pallas kernels: 0 us -> 48.2 us
  matrix products: 21.4 us -> 14.3 us
  blocking collectives: 44.9 us -> 41.9 us
    all_gather x1 -> x0, waiting for transfers between devices: 103 us -> none  [sent_together(): out = lax.all_gather(both, axis, axis=dim, tiled=True)]
    pallas_call x0 -> x1, Pallas kernels: none -> 48.2 us  [project(): pl.pallas_call(project_kernel, out_shape=(jax.ShapeDtypeStruct((NG, seq,...]
    all_gather x1, waiting for transfers between devices: 29 us -> 0.02 us  [gathered_by_axis(): value = lax.all_gather(value, axis, axis=dim, tiled=True)]
    dot_general x3 -> x0, matrix products: 6.14 us -> none  [on_device(): jnp.dot(normed, portion, preferred_element_type=jnp.float32)]
    all_to_all x2, blocking collectives: 12.3 us -> 9.14 us  [sent_to_all(): return lax.all_to_all(copies, axis, split_axis=0, concat_axis=0, tiled=True)]
  transfers between devices with their start and end apart: 5 -> 4, of which waited for: 4 -> 2; matrix products, arithmetic and copies ran while one was open for 8% -> 10% of each run, Pallas kernels for 0% -> 25%
where the time goes in v1:
time: 196 us; the launch traced here: 195 us
  Pallas kernels  48.2 us (25%)
  blocking collectives  41.9 us (21%)
  waiting for transfers between devices  38.7 us (20%)
  starting transfers between devices  20.9 us (11%)
  between operations  15 us (8%)
  matrix products  14.3 us (7%)
  other arithmetic  9.14 us (5%)
  local copies, waits for them, and re-layouts  6.95 us (4%)
    pallas_call x1, Pallas kernels, project(): pl.pallas_call(project_kernel, out_shape=(jax.ShapeDtypeStruct((NG, seq,...  48.2 us
    all_to_all x1, waiting for transfers between devices, on_device(): lax.all_to_all(outgoing, EP, split_axis=0, concat_axis=0, tiled=True)  25 us
    all_gather x2, blocking collectives, gathered_by_axis(): value = lax.all_gather(value, axis, axis=dim, tiled=True)  21.1 us
    all_to_all x1, waiting for transfers between devices, on_device(): lax.all_to_all(expert_sum.reshape(sources, held_slots, -1), EP, split_axi...  13.7 us
    all_to_all x1, starting transfers between devices, on_device(): lax.all_to_all(outgoing, EP, split_axis=0, concat_axis=0, tiled=True)  11.1 us
    all_to_all x2, blocking collectives, sent_to_all(): return lax.all_to_all(copies, axis, split_axis=0, concat_axis=0, tiled=True)  9.14 us
    all_to_all x1, blocking collectives, summed_on_arrival(): blocks = lax.all_to_all(split_up(value, dim, count), axis, 0, 0, tiled=True)  7.25 us
    all_to_all x1, starting transfers between devices, on_device(): lax.all_to_all(expert_sum.reshape(sources, held_slots, -1), EP, split_axi...  6.17 us
  transfers between devices with their start and end apart: 4, of which 2 were waited for; matrix products, arithmetic and copies ran while one was open for 10% of the time, Pallas kernels for 25%

profile of v1, /device:TPU:1, one launch (start us, length us, event | category | flops | bytes accessed | tf_op | source)
XLA Modules:
  0.0 195.1 jit_solution(1532385533809865774)
XLA Ops:
  7.2 10.5 %all_gather.12 = bf16[512,64]{0,1:T(8,128)(2,1)S(1)} all-gather(bf16[512,16]{0,1:T(8,128)(2,1)} %param.31), channel_id=1, replica_groups=mesh['ep_0'=8,'ep_1'=4,'ep_2'=4,'tp'=2] {'ep_2'}, dimensions={1}, use_global_device_ids=true | all-gather | bytes 81920 | tf_op jit(solution)/shard_map/all_gather | solution.py:27
  17.7 10.6 %all_gather.13 = bf16[512,256]{0,1:T(8,128)(2,1)} all-gather(bf16[512,64]{0,1:T(8,128)(2,1)S(1)} %all_gather.12), channel_id=1, replica_groups=mesh['ep_0'=8,'ep_1'=4,'ep_2'=4,'tp'=2] {'ep_1'}, dimensions={1}, use_global_device_ids=true | all-gather | bytes 327680 | tf_op jit(solution)/shard_map/all_gather | solution.py:27
  28.4 0.7 convert_element_type.110
  29.0 0.8 copy.71
  30.5 1.4 bitcast_bitcast_fusion.2.wsrc_ref
  31.9 48.2 %project.1 = (bf16[16,16,128]{2,1,0:T(8,128)(2,1)}, bf16[8,16,512]{2,1,0:T(8,128)(2,1)}) custom-call(bf16[16,2048]{1,0:T(8,128)(2,1)} %tokens_ref.1, f32[1,2048]{1,0:T(1,128)} %bitcast.86, bf16[16,16,128]{2,1,0:T(8,128)(2,1)} %bitcast_bitcast_fusion.2.wsrc_ref, bf16[16,512]{1,0:T(8,128)(2,1)} %bitcast.84), custom_call_target="tpu_custom_call" | custom-call | tf_op jit(solution)/shard_map/project/pallas_call | solution.py:308
  80.1 0.8 convert_bitcast_fusion
  81.7 2.8 %fusion.40 = f32[16,8,1,64]{3,2,1,0:T(1,128)S(1)} fusion(f32[16,8,64,1]{2,3,1,0:T(1,128)S(1)} %bitcast.80, f32[16,8,64,64]{3,2,1,0:T(8,128)} %param.22), kind=kOutput, calls=%fused_computation.84 | convolution fusion | flops 1048576 | bytes 2162688 | tf_op jit(solution)/shard_map/shd,shde->she/dot_general | solution.py:101
  85.1 2.2 %convolution_convert_fusion.3 = bf16[16,2048]{1,0:T(8,128)(2,1)S(1)} fusion(bf16[512,2048]{0,1:T(8,128)(2,1)} %all-gather.3.cloned.1.call-done, f32[16,512]{1,0:T(8,128)S(1)} %reshape.180, f32[4,2,8,128]{3,2,1,0:T(8,128)S(1)} %get-tuple-element.8), kind=kOutput, calls=%fused_computation.5 | convolution fusion | flops 33636352 | bytes 2228224 | tf_op jit(solution)/shard_map/dot_general | solution.py:369
  87.4 5.4 %all_to_all.30 = bf16[2,16,2048]{2,1,0:T(8,128)(2,1)S(1)} all-to-all(bf16[2,16,2048]{2,1,0:T(8,128)(2,1)S(1)} %broadcast_in_dim.15), channel_id=1, replica_groups=mesh['ep_0'=8,'ep_1'=4,'ep_2'=4,'tp'=2] {'tp'}, dimensions={0} | all-to-all | bytes 262144 | tf_op jit(solution)/shard_map/all_to_all | solution.py:33
  93.1 0.5 convolution_convert_fusion
  93.6 1.5 reshape.182
  95.1 11.1 %all-to-all-start.2 = ((bf16[128,2,2048]{2,1,0:T(2,128)(2,1)}), bf16[128,2,2048]{2,1,0:T(2,128)(2,1)S(1)}, u32[]{:S(2)}, u32[]{:S(2)}) async-start(bf16[128,2,2048]{2,1,0:T(2,128)(2,1)} %reshape.182), calls=%async_computation.2 | async-start | bytes 2097152 | tf_op jit(solution)/shard_map/all_to_all | solution.py:402
  106.2 1.5 fusion.39
  107.7 2.0 %convolution_convert_fusion.2 = bf16[16,2048]{1,0:T(8,128)(2,1)S(1)} fusion(bf16[256,2048]{1,0:T(8,128)(2,1)S(1)} %copy-done.1, bf16[2048,256]{1,0:T(8,128)(2,1)} %param.38, f32[16,256]{1,0:T(8,128)S(1)} %fusion.39, f32[2048]{0:T(1024)S(1)} %copy-done.3, f32[16]{0:T(128)S(1)} %add_rsqrt_fusion.2, bf16[16,2048]{1,0:T(8,128)(2,1)S(1)} %fusion.18), kind=kOutput, calls=%fused_computation.4 | convolution fusion | flops 33742848 | bytes 2252864 | tf_op jit(solution)/shard_map/dot_general | solution.py:421
  109.7 0.7 copy.90
  110.4 25.0 %all-to-all-done.2 = bf16[128,2,2048]{2,1,0:T(2,128)(2,1)S(1)} async-done(((bf16[128,2,2048]{2,1,0:T(2,128)(2,1)}), bf16[128,2,2048]{2,1,0:T(2,128)(2,1)S(1)}, u32[]{:S(2)}, u32[]{:S(2)}) %all-to-all-start.2) | async-done | bytes 1048608 | tf_op jit(solution)/shard_map/all_to_all | solution.py:402
  135.4 0.4 reshape.183
  135.8 2.4 %fusion.8 = f32[256,256]{1,0:T(8,128)} fusion(bf16[256,2048]{1,0:T(8,128)(2,1)S(1)} %reshape.183, bf16[1,2048,256]{2,1,0:T(8,128)(2,1)} %param.34), kind=kOutput, calls=%fused_computation.16 | convolution fusion | flops 268435456 | bytes 2359296 | tf_op jit(solution)/shard_map/dot_general | solution.py:407
  138.1 2.5 %convolution_convert_fusion.1 = bf16[256,2048]{1,0:T(8,128)(2,1)S(1)} fusion(bf16[256,2048]{1,0:T(8,128)(2,1)S(1)} %reshape.183, bf16[1,256,2048]{2,1,0:T(8,128)(2,1)S(1)} %copy-done, bf16[1,2048,256]{2,1,0:T(8,128)(2,1)} %param.35, f32[256,256]{1,0:T(8,128)} %fusion.8), kind=kOutput, calls=%fused_computation.3 | convolution fusion | flops 537788416 | bytes 4456448 | tf_op jit(solution)/shard_map/dot_general | solution.py:410
  140.8 7.3 %all_to_all.31 = bf16[2,256,1024]{2,1,0:T(8,128)(2,1)S(1)} all-to-all(bf16[2,256,1024]{2,1,0:T(8,128)(2,1)S(1)} %bitcast.78), channel_id=1, replica_groups=mesh['ep_0'=8,'ep_1'=4,'ep_2'=4,'tp'=2] {'tp'}, dimensions={0} | all-to-all | bytes 2097152 | tf_op jit(solution)/shard_map/all_to_all | solution.py:47
  148.1 3.7 %all-to-all-start.1 = ((bf16[2,16,1024]{2,1,0:T(8,128)(2,1)}), bf16[2,16,1024]{2,1,0:T(8,128)(2,1)S(1)}, u32[]{:S(2)}, u32[]{:S(2)}) async-start(bf16[2,16,1024]{2,1,0:T(8,128)(2,1)} %bitcast.77), calls=%async_computation.1 | async-start | bytes 131072 | tf_op jit(solution)/shard_map/all_to_all | solution.py:47
  151.7 0.2 reduce_sum.119
  152.0 1.0 reshape.185
  153.0 6.2 %all-to-all-start.4 = ((bf16[128,2,1024]{2,1,0:T(2,128)(2,1)}), bf16[128,2,1024]{2,1,0:T(2,128)(2,1)S(1)}, u32[]{:S(2)}, u32[]{:S(2)}) async-start(bf16[128,2,1024]{2,1,0:T(2,128)(2,1)} %reshape.185), calls=%async_computation.4 | async-start | bytes 1048576 | tf_op jit(solution)/shard_map/all_to_all | solution.py:412
  159.2 0.6 dynamic-slice
  160.5 4.3 %multiply_add_fusion = f32[16,8,64,64]{3,2,1,0:T(8,128)} fusion(f32[16,8,64,64]{3,2,1,0:T(8,128)} %param.22, f32[16,8,64]{2,1,0:T(8,128)S(1)} %reshape.190, f32[16,8,64]{2,1,0:T(8,128)S(1)} %get-tuple-element.21, f32[8]{0:T(128)S(1)} %dynamic_slice.9), kind=kLoop, calls=%fused_computation.1 | loop fusion | flops 1572864 | bytes 4259872 | tf_op jit(solution)/shard_map/add | solution.py:105
  164.8 13.7 %all-to-all-done.4 = bf16[128,2,1024]{2,1,0:T(2,128)(2,1)S(1)} async-done(((bf16[128,2,1024]{2,1,0:T(2,128)(2,1)}), bf16[128,2,1024]{2,1,0:T(2,128)(2,1)S(1)}, u32[]{:S(2)}, u32[]{:S(2)}) %all-to-all-start.4) | async-done | bytes 524320 | tf_op jit(solution)/shard_map/all_to_all | solution.py:412
  178.7 0.3 multiply_reduce_fusion.1
  179.3 4.4 %all-reduce = f32[32]{0:T(128)S(1)} all-reduce(f32[32]{0:T(128)S(1)} %dynamic-update-slice), channel_id=2, replica_groups=mesh['ep_0'=8,'ep_1'=4,'ep_2'=4,'tp'=2] {'tp'}, use_global_device_ids=true, to_apply=%add | all-reduce | flops 32 | bytes 256
  183.9 3.8 %all_to_all.32 = bf16[2,16,1024]{2,1,0:T(8,128)(2,1)S(1)} all-to-all(bf16[2,16,1024]{2,1,0:T(8,128)(2,1)S(1)} %broadcast_in_dim.18), channel_id=1, replica_groups=mesh['ep_0'=8,'ep_1'=4,'ep_2'=4,'tp'=2] {'tp'}, dimensions={0} | all-to-all | bytes 131072 | tf_op jit(solution)/shard_map/all_to_all | solution.py:33
  187.7 0.6 copy.81
  (65 shorter events, 3.2 us)
Async XLA Ops:
  7.2 131.0 %copy-start = (bf16[1,256,2048]{2,1,0:T(8,128)(2,1)S(1)}, bf16[1,256,2048]{2,1,0:T(8,128)(2,1)}, u32[]{:S(2)}) copy-start(bf16[1,256,2048]{2,1,0:T(8,128)(2,1)} %param.36) | copy-start | bytes 3145732
  7.2 77.8 %copy-start.4 = (s32[16,6]{0,1:T(8,128)S(1)}, s32[16,6]{0,1:T(8,128)}, u32[]{:S(2)}) copy-start(s32[16,6]{0,1:T(8,128)} %param.32) | copy-start | bytes 1156
  7.2 77.9 %all-gather.3.cloned.1.call-start = ((), (), s32[]{:S(2)}) async-start(), calls=%async_computation.6 | async-start | bytes 2359296 | tf_op jit(solution)/shard_map/all_gather | solution.py:27
  81.6 11.3 %copy-start.2 = (bf16[16,2048]{1,0:T(8,128)(2,1)S(1)}, bf16[16,2048]{1,0:T(8,128)(2,1)}, u32[]{:S(2)}) copy-start(bf16[16,2048]{1,0:T(8,128)(2,1)} %tokens_ref.1) | copy-start | bytes 196612
  81.6 11.3 %copy-start.5 = (f32[2048]{0:T(1024)S(1)}, f32[2048]{0:T(1024)}, u32[]{:S(2)}) copy-start(f32[2048]{0:T(1024)} %param.24) | copy-start | bytes 24580
  81.6 11.5 %copy-start.3 = (f32[2048]{0:T(1024)S(1)}, f32[2048]{0:T(1024)}, u32[]{:S(2)}) copy-start(f32[2048]{0:T(1024)} %param.25) | copy-start | bytes 24580
  87.3 20.4 %copy-start.1 = (bf16[256,2048]{1,0:T(8,128)(2,1)S(1)}, bf16[256,2048]{1,0:T(8,128)(2,1)}, u32[]{:S(2)}) copy-start(bf16[256,2048]{1,0:T(8,128)(2,1)} %param.39) | copy-start | bytes 3145732
  95.1 40.2 %all-to-all-start.2 = ((bf16[128,2,2048]{2,1,0:T(2,128)(2,1)}), bf16[128,2,2048]{2,1,0:T(2,128)(2,1)S(1)}, u32[]{:S(2)}, u32[]{:S(2)}) async-start(bf16[128,2,2048]{2,1,0:T(2,128)(2,1)} %reshape.182), calls=%async_computation.2 | async-start | bytes 2097152 | tf_op jit(solution)/shard_map/all_to_all | solution.py:402
  140.7 18.5 %copy-start.7 = (u32[256]{0:T(256)S(1)}, u32[256]{0:T(256)}, u32[]{:S(2)}) copy-start(u32[256]{0:T(256)} %constant.78) | copy-start | bytes 3076
  140.7 19.7 %copy-start.6 = (f32[16,6]{0,1:T(8,128)S(1)}, f32[16,6]{0,1:T(8,128)}, u32[]{:S(2)}) copy-start(f32[16,6]{0,1:T(8,128)} %param.33) | copy-start | bytes 1156
  148.1 4.9 %all-to-all-start.1 = ((bf16[2,16,1024]{2,1,0:T(8,128)(2,1)}), bf16[2,16,1024]{2,1,0:T(8,128)(2,1)S(1)}, u32[]{:S(2)}, u32[]{:S(2)}) async-start(bf16[2,16,1024]{2,1,0:T(8,128)(2,1)} %bitcast.77), calls=%async_computation.1 | async-start | bytes 131072 | tf_op jit(solution)/shard_map/all_to_all | solution.py:47
  153.0 25.6 %all-to-all-start.4 = ((bf16[128,2,1024]{2,1,0:T(2,128)(2,1)}), bf16[128,2,1024]{2,1,0:T(2,128)(2,1)S(1)}, u32[]{:S(2)}, u32[]{:S(2)}) async-start(bf16[128,2,1024]{2,1,0:T(2,128)(2,1)} %reshape.185), calls=%async_computation.4 | async-start | bytes 1048576 | tf_op jit(solution)/shard_map/all_to_all | solution.py:412
  160.5 23.3 %dynamic-slice-start = ((f32[2048]{0:T(1024)}, s32[]{:T(128)}), f32[1024]{0:T(1024)S(1)}, s32[]{:S(2)}) async-start(f32[2048]{0:T(1024)} %param.26, s32[]{:T(128)} %select_n.12), calls=%async_computation.7 | async-start | bytes 8704 | tf_op jit(solution)/shard_map/dynamic_slice | solution.py:427
Sparse Core Ops, SparseCore 0:
  28.5 55.7 all-gather.2

commit v2 on v1

v2 whole, which is shorter than its diff:
```python
import jax
import jax.numpy as jnp
import numpy as np
from jax import lax
from jax.experimental import pallas as pl
from jax.experimental.pallas import tpu as pltpu
from jax.sharding import Mesh
from jax.sharding import PartitionSpec as P

HEAD = 64
HEADS = 16
EP = ("ep_0", "ep_1", "ep_2")
EPS = 1e-06
THETA = 10000.0
MESH = pl.DeviceIdType.MESH
NZ, NY, NX, NG = 8, 4, 4, 16
BF16 = jnp.bfloat16
F32 = jnp.float32


def place():
    z, y, x, c = (lax.axis_index(name) for name in ("ep_0", "ep_1", "ep_2", "tp"))
    return z, y * NX + x, c


def device(z, g, c):
    return (z, g // NX, g % NX, c)


def remote(src, dst, send_sem, recv_sem, target):
    return pltpu.make_async_remote_copy(
        src_ref=src,
        dst_ref=dst,
        send_sem=send_sem,
        recv_sem=recv_sem,
        device_id=target,
        device_id_type=MESH,
    )


def each(low, high, body):
    def step(i, carry):
        body(i)
        return carry

    lax.fori_loop(low, high, step, 0)


def dot(a, b, dims=((1,), (0,))):
    return lax.dot_general(a, b, (dims, ((), ())), preferred_element_type=F32)


def wide_rows(blocks):
    rows = blocks.shape[0] * blocks.shape[2]
    return jnp.concatenate(
        [blocks[:, k].reshape(rows, 128) for k in range(blocks.shape[1])], axis=1
    )


def row_scale(blocks):
    count = blocks.shape[0] * blocks.shape[2]
    total = jnp.sum(jnp.sum(blocks * blocks, axis=0), axis=-1, keepdims=True)
    return lax.rsqrt(total / count + EPS)[None]


class Group:
    def __init__(self, me, size, at, src, dst, send, recv):
        self.me, self.size, self.at, self.src, self.dst = me, size, at, src, dst
        self.send, self.recv = send, recv

    def out(self, i):
        k = (self.me + i) % self.size
        return remote(
            self.src(k), self.dst(self.me), self.send.at[k], self.recv.at[self.me], self.at(k)
        )

    def come(self, i):
        k = (self.me + i) % self.size
        return remote(
            self.src(k), self.dst(k), self.send.at[k], self.recv.at[k], self.at(k)
        )

    def start(self):
        each(1, self.size, lambda i: self.out(i).start())

    def wait(self):
        each(1, self.size, lambda i: self.come(i).wait_recv())

    def drain(self):
        each(1, self.size, lambda i: self.out(i).wait_send())


def layer_kernel(
    tokens_ref, mix_ref, post_ref, ffn_ref, outg_ref, wsrc_ref, wot_ref, cos_ref, sin_ref, dec_ref, rt_ref,
    state_hbm, eg_hbm, eu_hbm, ed_hbm, sg_hbm, su_hbm, sd_hbm,
    result_ref, new_hbm,
    state, eg, eu, ed, sg, su, sd,
    tbuf, abuf, wbuf, zbuf, wo, xsend, xbuf, osend, obuf, qbuf, onehot, comb_hi, comb_lo,
    kt, vsc, fs, rbuf, psend, pbuf, middle, mo, mbuf, shs, shb, ysend, ebuf, dsend, dbuf, ret, back,
    csend, cbuf, mixs, mixb,
    l_s, w_s, a_s, a_r, t_s, t_r, b_s, b_r, c_s, c_r, d_s, d_r, q_s, q_r, o_s, o_r, r_s, r_r,
    p_s, p_r, m_s, m_r, y_s, y_r, f_s, f_r, g_s, g_r, h_s, h_r, x_s, x_r,
):
    z, g, c = place()
    loads = [
        pltpu.make_async_copy(src, dst, w_s.at[i])
        for i, (src, dst) in enumerate(
            ((state_hbm, state), (sg_hbm, sg), (su_hbm, su), (sd_hbm, sd),
             (eg_hbm, eg), (eu_hbm, eu), (ed_hbm, ed))
        )
    ]
    barrier = pltpu.get_barrier_semaphore()

    def greet_plane(i):
        other = (g * 2 + c + i) % (2 * NG)
        pl.semaphore_signal(
            barrier, inc=1, device_id=device(z, other // 2, other % 2), device_id_type=MESH
        )

    def greet_column(i):
        other = (z + 1 + i // 2) % NZ
        pl.semaphore_signal(
            barrier, inc=1, device_id=device(other, g, i % 2), device_id_type=MESH
        )

    each(1, 2 * NG, greet_plane)
    each(0, 2 * NZ - 2, greet_column)
    for load in loads:
        load.start()

    half = tbuf.shape[-1]
    wide = tokens_ref[...].astype(F32)
    scale = lax.rsqrt(jnp.mean(wide * wide, axis=-1, keepdims=True) + EPS)
    cols = pl.ds(pl.multiple_of(c * half, 128), half)
    part = tokens_ref[:, cols].astype(F32)
    tbuf[pl.ds(g, 1)] = (part * scale * mix_ref[:, cols]).astype(BF16)[None]
    pl.semaphore_wait(barrier, 2 * NG - 1 + 2 * NZ - 2)

    def plane(src, dst, send, recv):
        return Group(g, NG, lambda k: device(z, k, c), src, dst, send, recv)

    def column(src, dst, send, recv):
        return Group(z, NZ, lambda k: device(k, g, c), src, dst, send, recv)

    ga = plane(lambda k: wsrc_ref.at[k], lambda k: abuf.at[k], a_s, a_r)
    gt = plane(lambda k: tbuf.at[g], lambda k: tbuf.at[k], t_s, t_r)
    gc = column(lambda k: wot_ref, lambda k: zbuf.at[k], c_s, c_r)
    gq = column(lambda k: rt_ref, lambda k: qbuf.at[k], q_s, q_r)
    ga.start()
    own_a = pltpu.make_async_copy(wsrc_ref.at[g], abuf.at[g], l_s.at[0])
    own_a.start()
    gt.start()
    gc.start()
    gq.start()
    own_z = pltpu.make_async_copy(wot_ref, zbuf.at[z], l_s.at[1])
    own_z.start()
    qbuf[pl.ds(z, 1)] = rt_ref[...][None]

    ga.wait()
    own_a.wait()
    b_core = z // (NZ // 2)

    def b_copy(j):
        other = (z + j) % NZ
        return remote(
            abuf, wbuf.at[c, z % 4], b_s.at[j], b_r.at[c, z % 4], device(other, g, b_core)
        )

    each(1, NZ, lambda j: b_copy(j).start())

    @pl.when(b_core == c)
    def _():
        pltpu.make_async_copy(abuf, wbuf.at[c, z % 4], b_r.at[c, z % 4]).start()

    @pl.when(b_core != c)
    def _():
        b_copy(0).start()

    gc.wait()
    own_z.wait()
    to_half = g // (NG // 2)

    def d_copy(k):
        other = 2 * k + to_half
        return other, remote(
            zbuf.at[k], wo.at[g % 8], d_s.at[k], d_r.at[g % 8], device(z, other, c)
        )

    def d_start(k):
        other, copy = d_copy(k)

        @pl.when(other == g)
        def _():
            pltpu.make_async_copy(zbuf.at[k], wo.at[g % 8], d_r.at[g % 8]).start()

        @pl.when(other != g)
        def _():
            copy.start()

    each(0, NZ, d_start)

    gq.wait()
    routing = qbuf[...].reshape(NZ * 16, 128)
    slots = 16 * NG
    row_z = lax.broadcasted_iota(jnp.int32, (NZ * 16, slots), 0) // 16
    lane = lax.broadcasted_iota(jnp.int32, (NZ * 16, slots), 1)
    slot_id = ((z * NG + lane // 16) * 2 + lane % 2).astype(F32)
    same_z = row_z == (lane % 16) // 2
    named = jnp.zeros((NZ * 16, slots), F32)
    weight = jnp.zeros((NZ * 16, slots), F32)
    for k in range(6):
        hit = jnp.logical_and(routing[:, k : k + 1] == slot_id, same_z)
        named = named + jnp.where(hit, 1.0, 0.0)
        weight = weight + jnp.where(hit, routing[:, 8 + k : 9 + k], 0.0)
    onehot[...] = named.T.astype(BF16)
    upper = weight.astype(BF16)
    comb_hi[...] = upper
    comb_lo[...] = (weight - upper.astype(F32)).astype(BF16)

    gt.wait()

    def b_wait(j):
        pltpu.make_async_copy(abuf, wbuf.at[j // 4, j % 4], b_r.at[j // 4, j % 4]).wait()

    each(0, NZ, b_wait)
    rows = NG * tbuf.shape[1]
    normed = tbuf[...].reshape(rows, half)

    def weights(k):
        return wbuf[pl.ds(k, 1)].reshape(half, 128)

    xsend[...] = dot(normed, weights(1 - c))
    swap = remote(xsend, xbuf, x_s.at[0], x_r.at[0], device(z, g, 1 - c))
    swap.start()
    mine = dot(normed, weights(c))
    swap.wait_recv()
    osend[...] = (mine + xbuf[...]).astype(BF16).reshape(osend.shape)
    go = plane(lambda k: osend.at[k], lambda k: obuf.at[k], o_s, o_r)
    go.start()
    obuf[pl.ds(g, 1)] = osend[pl.ds(g, 1)]
    loads[0].wait()
    fs[...] = jnp.zeros_like(fs)
    go.wait()

    low_half = lax.broadcasted_iota(jnp.int32, (16, 128), 1) < 64
    first = lax.broadcasted_iota(jnp.int32, (16, 128), 1) % 64 < 32

    def rotate(v):
        other = jnp.where(first, pltpu.roll(v, 96, 1), pltpu.roll(v, 32, 1))
        return v * cos_ref[...] + other * sin_ref[...]

    def by_head(v):
        low = jnp.sum(jnp.where(low_half, v, 0.0), axis=-1, keepdims=True)
        high = jnp.sum(jnp.where(low_half, 0.0, v), axis=-1, keepdims=True)
        return jnp.where(low_half, low, high)

    def read_pair(hp):
        def block(k):
            return obuf[pl.ds(4 * k + hp, 1)][0].astype(F32)

        query = rotate(block(0))
        key = rotate(block(1)) * HEAD ** (-0.5)
        value = block(2)
        query_t = query.T
        kt[pl.ds(hp, 1)] = key.T[None]
        vsc[pl.ds(2 * hp, 1)] = value[None]
        vsc[pl.ds(2 * hp + 1, 1)] = pltpu.roll(value, 64, 1)[None]
        for h in range(2):
            for s in range(16):
                held = state[s, pl.ds(2 * hp + h, 1)][0]
                column_q = query_t[h * 64 : (h + 1) * 64, s : s + 1]
                fs[h, s : s + 1, 0:64] = jnp.sum(column_q * held, axis=0, keepdims=True)
        from_state = jnp.where(low_half, fs[0], pltpu.roll(fs[1], 64, 1))
        decay = jnp.where(
            low_half[0:1], dec_ref[c, pl.ds(2 * hp, 1)], dec_ref[c, pl.ds(2 * hp + 1, 1)]
        )
        read = decay * from_state + by_head(query * key) * value
        read = read * lax.rsqrt(by_head(read * read) / HEAD + EPS)
        rbuf[pl.ds(g, 1), pl.ds(hp, 1)] = (read * jax.nn.silu(block(3))).astype(BF16)[None, None]

    each(0, 4, read_pair)
    gr = plane(lambda k: rbuf.at[g], lambda k: rbuf.at[k], r_s, r_r)
    gr.start()

    def update_pair(hp):
        keys = kt[pl.ds(hp, 1)][0]
        for h in range(2):
            decay = dec_ref[c, pl.ds(2 * hp + h, 1)][:, 0:64]
            value = vsc[pl.ds(2 * hp + h, 1)][0]
            for s in range(16):
                held = state[s, pl.ds(2 * hp + h, 1)][0]
                column_k = keys[h * 64 : (h + 1) * 64, s : s + 1]
                state[s, pl.ds(2 * hp + h, 1)] = (
                    decay * held + column_k * value[s : s + 1, 0:64]
                )[None]

    each(0, 4, update_pair)
    store = pltpu.make_async_copy(state, new_hbm, w_s.at[7])
    store.start()

    def d_wait(k):
        pltpu.make_async_copy(zbuf.at[k], wo.at[k], d_r.at[k]).wait()

    each(0, NZ, d_wait)
    gr.wait()

    partial = dot(wide_rows(rbuf[...]), wo[...].reshape(128, 512), ((1,), (1,)))
    psend[...] = partial.astype(BF16).reshape(psend.shape)
    gp = [
        plane(lambda k: psend.at[k], lambda k: pbuf.at[c, k], p_s.at[0], p_r.at[c]),
    ]
    gp[0].start()
    gp_other = Group(
        g, NG, lambda k: device(z, k, 1 - c), lambda k: psend.at[k], lambda k: pbuf.at[c, k],
        p_s.at[1], p_r.at[c],
    )
    each(0, NG, lambda i: gp_other.out(i).start())
    pbuf[pl.ds(c, 1), pl.ds(g, 1)] = psend[pl.ds(g, 1)][None]
    gp[0].wait()
    gp_from = Group(
        g, NG, lambda k: device(z, k, 1 - c), lambda k: psend.at[k], lambda k: pbuf.at[1 - c, k],
        p_s.at[1], p_r.at[1 - c],
    )
    each(0, NG, lambda i: gp_from.come(i).wait_recv())
    mixed = (pbuf[0].astype(F32) + pbuf[1].astype(F32)).astype(BF16).astype(F32)
    tok = jnp.stack([tokens_ref[:, k * 128 : (k + 1) * 128] for k in range(NG)]).astype(F32)
    mid = (tok + mixed * row_scale(mixed) * post_ref[...]).astype(BF16)
    middle[...] = mid
    mid = mid.astype(F32)
    mo[...] = (mid * row_scale(mid) * ffn_ref[...]).astype(BF16)

    own_blocks = pl.ds(pl.multiple_of(c * 8, 8), 8)
    mbuf[pl.ds(z, 1)] = mo[own_blocks][None]
    gm = column(lambda k: mbuf.at[z], lambda k: mbuf.at[k], m_s, m_r)
    gm.start()
    for load in loads[1:4]:
        load.wait()
    rows_in = wide_rows(mo[...][None])
    shared_hidden = (jax.nn.silu(dot(rows_in, sg[...])) * dot(rows_in, su[...])).astype(BF16)
    shared_part = dot(shared_hidden, sd[...]).astype(BF16)
    parts = jnp.stack([shared_part[:, k * 128 : (k + 1) * 128] for k in range(NG)])
    shs[...] = parts.reshape(shs.shape)
    share = remote(shs.at[1 - c], shb, x_s.at[1], x_r.at[1], device(z, g, 1 - c))
    share.start()
    for load in loads[4:]:
        load.wait()
    gm.wait()
    sorted_rows = dot(onehot[...], wide_rows(mbuf[...])).astype(BF16)
    for k in range(8):
        ysend[:, k] = sorted_rows[:, k * 128 : (k + 1) * 128].reshape(NG, 16, 128)
    gy = plane(lambda k: ysend.at[k], lambda k: ebuf.at[c, k], y_s, y_r)
    gy.start()
    ebuf[pl.ds(c, 1), pl.ds(g, 1)] = ysend[pl.ds(g, 1)][None]

    def forward(half_from, k):
        return remote(
            ebuf.at[half_from, k], ebuf.at[half_from, k], f_s.at[k], f_r.at[k], device(z, g, 1 - c)
        )

    forward(c, g).start()

    def relay(i):
        gy.come(i).wait_recv()
        forward(c, (g + i) % NG).start()

    each(1, NG, relay)

    def expert_in(k):
        blocks = wide_rows(ebuf[pl.ds(k, 1)][0])
        rows_of = pl.ds(pl.multiple_of(k * half, 128), half)
        return dot(blocks, eg[0, rows_of]), dot(blocks, eu[0, rows_of])

    gate_c, up_c = expert_in(c)
    each(0, NG, lambda k: forward(1 - c, k).wait_recv())
    gate_o, up_o = expert_in(1 - c)
    hidden = (jax.nn.silu(gate_c + gate_o) * (up_c + up_o)).astype(BF16)

    def down(k):
        out = dot(hidden, ed[0, :, pl.ds(pl.multiple_of(k * half, 128), half)]).astype(BF16)
        return [out[:, j * 128 : (j + 1) * 128].reshape(NG, 16, 128) for j in range(8)]

    for j, block in enumerate(down(1 - c)):
        dsend[:, j] = block
    give = remote(dsend, dbuf, x_s.at[2], x_r.at[2], device(z, g, 1 - c))
    give.start()
    kept = down(c)
    give.wait_recv()
    for j in range(8):
        ret[:, j] = (kept[j].astype(F32) + dbuf[:, j].astype(F32)).astype(BF16)
    gg = plane(lambda k: ret.at[k], lambda k: back.at[k], g_s, g_r)
    gg.start()
    back[pl.ds(g, 1)] = ret[pl.ds(g, 1)]
    share.wait_recv()
    shared_out = (shs[pl.ds(c, 1)][0].astype(F32) + shb[...].astype(F32)).astype(BF16).astype(F32)
    gg.wait()

    answers = wide_rows(back[...])
    sums = (dot(comb_hi[...], answers) + dot(comb_lo[...], answers)).astype(BF16)
    for k in range(8):
        csend[:, k] = sums[:, k * 128 : (k + 1) * 128].reshape(NZ, 16, 128)
    gh = column(lambda k: csend.at[k], lambda k: cbuf.at[k], h_s, h_r)
    gh.start()
    cbuf[pl.ds(z, 1)] = csend[pl.ds(z, 1)]
    gh.wait()
    mixs[...] = shared_out + jnp.sum(cbuf[...].astype(F32), axis=0)
    last = remote(mixs, mixb, x_s.at[3], x_r.at[3], device(z, g, 1 - c))
    last.start()
    last.wait_recv()
    first_half = jnp.where(c == 0, mixs[...], mixb[...])
    second_half = jnp.where(c == 0, mixb[...], mixs[...])
    mixture = jnp.concatenate([first_half, second_half], axis=0)
    final = (middle[...].astype(F32) + mixture * row_scale(mixture) * outg_ref[...]).astype(BF16)
    for k in range(NG):
        result_ref[:, k * 128 : (k + 1) * 128] = final[k]

    for group in (ga, gt, gc, gq, go, gr, gp[0], gm, gy, gg, gh):
        group.drain()
    each(0, NG, lambda i: gp_other.out(i).wait_send())
    each(1, NZ, lambda j: b_copy(j).wait_send())

    @pl.when(b_core != c)
    def _():
        b_copy(0).wait_send()

    def d_sent(k):
        other, copy = d_copy(k)

        @pl.when(other != g)
        def _():
            copy.wait_send()

    each(0, NZ, d_sent)
    each(0, NG, lambda k: forward(c, k).wait_send())
    for copy in (swap, share, give, last):
        copy.wait_send()
    store.wait()


def decay_table(head_count):
    head_order = np.arange(head_count, dtype=np.float32)
    decays = (1.0 - np.exp2(-5.0 - 7.0 * head_order / (head_count - 1))).astype(np.float32)
    return np.broadcast_to(decays.reshape(2, -1, 1), (2, head_count // 2, 128))


def on_device(
    tokens, lengths, prior_state, mix_gain, post_gain, ffn_gain, out_gain,
    query_weight, key_weight, value_weight, gate_weight, out_weight, routes, route_gates,
    expert_gate, expert_up, expert_down, shared_gate, shared_up, shared_down,
):
    seq, width = tokens.shape
    half_dim = HEAD // 2
    frequency = THETA ** (-jnp.arange(half_dim, dtype=F32) / half_dim)
    angles = lengths.astype(F32)[:, None] * frequency[None, :]
    cosine, sine = jnp.cos(angles), jnp.sin(angles)
    cos_table = jnp.concatenate([cosine] * 4, axis=1)
    sin_table = jnp.concatenate([-sine, sine] * 2, axis=1)
    earlier = jnp.arange(seq)[None, None, :, None] < jnp.arange(seq)[:, None, None, None]
    same = routes[:, :, None, None] == routes[None, None]
    rank = jnp.any(jnp.logical_and(same, earlier), axis=(2, 3)).astype(jnp.int32)
    slot = (routes * 2 + rank).astype(F32)
    gap = jnp.zeros((seq, 2), F32)
    table = jnp.concatenate([slot, gap, route_gates, jnp.zeros((seq, 114), F32)], axis=1)
    wsrc = jnp.concatenate((query_weight, key_weight, value_weight, gate_weight), axis=1)
    wsrc = wsrc.reshape(seq, NG, 128).transpose(1, 0, 2)
    dma = pltpu.SemaphoreType.DMA
    blocks = pltpu.VMEM((NG, 16, 128), BF16)
    halves = pltpu.VMEM((NG, 8, 16, 128), BF16)
    square = pltpu.VMEM((NG * seq, 128), F32)
    vmem = pl.BlockSpec(memory_space=pltpu.VMEM)
    anywhere = pl.BlockSpec(memory_space=pl.ANY)
    big = (prior_state, expert_gate, expert_up, expert_down, shared_gate, shared_up, shared_down)
    plane_sems, column_sems = dma((NG,)), dma((NZ,))
    return pl.pallas_call(
        layer_kernel,
        out_shape=(
            jax.ShapeDtypeStruct((seq, width), BF16),
            jax.ShapeDtypeStruct(prior_state.shape, F32),
        ),
        in_specs=[vmem] * 11 + [anywhere] * 7,
        out_specs=(vmem, anywhere),
        scratch_shapes=[
            *(pltpu.VMEM(array.shape, array.dtype) for array in big),
            pltpu.VMEM((NG, seq, width // 2), BF16),
            blocks,
            pltpu.VMEM((2, 4, NG, 16, 128), BF16),
            pltpu.VMEM((8, 16, 512), BF16),
            pltpu.VMEM((8, 16, 512), BF16),
            square,
            square,
            blocks,
            blocks,
            pltpu.VMEM((NZ, 16, 128), F32),
            pltpu.VMEM((16 * NG, 16 * NZ), BF16),
            pltpu.VMEM((16 * NZ, 16 * NG), BF16),
            pltpu.VMEM((16 * NZ, 16 * NG), BF16),
            pltpu.VMEM((4, 128, 16), F32),
            pltpu.VMEM((8, 16, 128), F32),
            pltpu.VMEM((2, 16, 128), F32),
            pltpu.VMEM((NG, 4, 16, 128), BF16),
            blocks,
            pltpu.VMEM((2, NG, 16, 128), BF16),
            blocks,
            blocks,
            pltpu.VMEM((NZ, 8, 16, 128), BF16),
            pltpu.VMEM((2, 8, 16, 128), BF16),
            pltpu.VMEM((8, 16, 128), BF16),
            halves,
            pltpu.VMEM((2, NG, 8, 16, 128), BF16),
            halves,
            halves,
            halves,
            halves,
            pltpu.VMEM((NZ, 8, 16, 128), BF16),
            pltpu.VMEM((NZ, 8, 16, 128), BF16),
            pltpu.VMEM((8, 16, 128), F32),
            pltpu.VMEM((8, 16, 128), F32),
            dma((2,)),
            dma((8,)),
            plane_sems, plane_sems,
            plane_sems, plane_sems,
            column_sems, dma((2, 4)),
            column_sems, column_sems,
            column_sems, column_sems,
            column_sems, column_sems,
            plane_sems, plane_sems,
            plane_sems, plane_sems,
            dma((2, NG)), dma((2, NG)),
            column_sems, column_sems,
            plane_sems, plane_sems,
            plane_sems, plane_sems,
            plane_sems, plane_sems,
            column_sems, column_sems,
            dma((4,)), dma((4,)),
        ],
        compiler_params=pltpu.CompilerParams(collective_id=0, has_side_effects=True),
        name="layer",
    )(
        tokens,
        mix_gain[None],
        *(gain.reshape(NG, 1, 128) for gain in (post_gain, ffn_gain, out_gain)),
        wsrc,
        out_weight.T,
        cos_table,
        sin_table,
        jnp.asarray(decay_table(HEADS)),
        table,
        *big,
    )


def solution(mesh):
    finer = Mesh(mesh.devices.reshape(8, 4, 4, mesh.shape["tp"]), ("ep_0", "ep_1", "ep_2", "tp"))
    in_specs = (
        P(EP, None),
        P(EP),
        P(EP, "tp", None, None),
        P(),
        P(),
        P(),
        P(),
        P(EP, "tp"),
        P(EP, "tp"),
        P(EP, "tp"),
        P(EP, "tp"),
        P("tp", EP),
        P(EP, None),
        P(EP, None),
        P(EP, None, "tp"),
        P(EP, None, "tp"),
        P(EP, "tp", None),
        P(None, "tp"),
        P(None, "tp"),
        P("tp", None),
    )
    out_specs = (P(EP, None), P(EP, "tp", None, None))
    return jax.shard_map(
        on_device, mesh=finer, in_specs=in_specs, out_specs=out_specs, check_vma=False
    )
```

time: 196 us -> 111 us (0.57)
  Pallas kernels: 48.2 us -> 95.9 us
  blocking collectives: 41.9 us -> 0 us
  waiting for transfers between devices: 38.7 us -> 0 us
  starting transfers between devices: 20.9 us -> 0 us
  between operations: 15 us -> 0.65 us
  matrix products: 14.3 us -> 0 us
  other arithmetic: 9.14 us -> 4.61 us
  local copies, waits for them, and re-layouts: 6.95 us -> 9.39 us
    pallas_call x1, Pallas kernels: 48.2 us -> 95.9 us  [on_device(): pl.pallas_call(layer_kernel, out_shape=(jax.ShapeDtypeStruct((seq, width)...]
    all_to_all x3 -> x0, waiting for transfers between devices: 38.7 us -> none  [the longest x1 25 us: on_device(): lax.all_to_all(outgoing, EP, split_axis=0, concat_axis=0, tiled=True)]
    all_gather x2 -> x0, blocking collectives: 21.1 us -> none  [gathered_by_axis(): value = lax.all_gather(value, axis, axis=dim, tiled=True)]
    all_to_all x3 -> x0, starting transfers between devices: 20.9 us -> none  [the longest x1 11.1 us: on_device(): lax.all_to_all(outgoing, EP, split_axis=0, concat_axis=0, tiled=True)]
    all_to_all x3 -> x0, blocking collectives: 16.4 us -> none  [the longest x2 9.14 us: sent_to_all(): return lax.all_to_all(copies, axis, split_axis=0, concat_axis=0, tiled=True)]
    dot_general x8 -> x0, matrix products: 14.3 us -> none  [the longest x1 2.85 us: retain(): from_state = jnp.einsum('shd,shde->she', rot_query, prior_state)]
    unnamed x20 -> x4, local copies, waits for them, and re-layouts: 1.64 us -> 7.79 us
    reshape x8 -> x0, local copies, waits for them, and re-layouts: 4.55 us -> none  [the longest x1 1.5 us: on_device(): outgoing = outgoing.reshape(experts_all, capacity, model_width)]
  transfers between devices with their start and end apart: 4 -> 0, of which waited for: 2 -> 0; matrix products, arithmetic and copies ran while one was open for 10% -> 0% of each run, Pallas kernels for 25% -> 0%
where the time goes in v2:
time: 111 us
  Pallas kernels  95.9 us (86%)
  local copies, waits for them, and re-layouts  9.39 us (8%)
  other arithmetic  4.61 us (4%)
    pallas_call x1, Pallas kernels, on_device(): pl.pallas_call(layer_kernel, out_shape=(jax.ShapeDtypeStruct((seq, width)...  95.9 us
    unnamed x4, local copies, waits for them, and re-layouts  7.79 us

profile of v2, /device:TPU:1, one launch (start us, length us, event | category | flops | bytes accessed | tf_op | source)
XLA Modules:
  0.0 110.6 jit_solution(8881096654497032320)
XLA Ops:
  0.6 0.7 convert_element_type.9
  1.3 0.1 pad.3.clone
  1.4 0.1 pad.1.clone
  1.5 1.0 and_reduce_fusion
  2.5 0.1 copy.39
  2.6 0.8 copy.40
  3.4 0.8 copy.37
  4.1 0.7 maximum_maximum_fusion.rt_ref
  4.8 0.1 fusion
  4.9 0.7 pad_maximum_fusion
  5.6 1.4 %bitcast_bitcast_fusion.wsrc_ref = bf16[16,16,128]{2,1,0:T(8,128)(2,1)} fusion(bf16[16,512]{1,0:T(8,128)(2,1)} %param.31, bf16[16,512]{1,0:T(8,128)(2,1)} %param.30, bf16[16,512]{1,0:T(8,128)(2,1)} %param.29, bf16[16,512]{1,0:T(8,128)(2,1)} %param.28), kind=kLoop, calls=%fused_computation.1 | loop fusion | flops 262144 | bytes 131072 | tf_op jit(solution)/shard_map/transpose | solution.py:464
  7.0 1.3 %jit_solution_.3.dec_ref = f32[2,8,128]{2,1,0:T(8,128)} broadcast(f32[2,8]{1,0:T(2,128)} %constant.14.clone), dimensions={0,1} | broadcast | bytes 8256 | tf_op jit(solution)
  8.4 95.9 %layer.1 = (bf16[16,2048]{1,0:T(8,128)(2,1)}, f32[16,8,64,64]{3,2,1,0:T(8,128)}) custom-call(bf16[16,2048]{1,0:T(8,128)(2,1)} %tokens_ref.1, f32[1,2048]{1,0:T(1,128)} %bitcast.13, f32[16,1,128]{2,1,0:T(1,128)} %bitcast.14, f32[16,1,128]{2,1,0:T(1,128)} %bitcast.15, f32[16,1,128]{2,1,0:T(1,128)} %bitcast.16, ...), custom_call_target="tpu_custom_call" | custom-call | tf_op jit(solution)/shard_map/layer/pallas_call | solution.py:473
  104.3 1.5 %copy.45 = bf16[16,2048]{1,0:T(8,128)(2,1)} copy(bf16[16,2048]{1,0:T(8,128)(2,1)} %get-tuple-element.9) | data formatting | bytes 131072
  105.8 4.8 %copy.46 = f32[16,8,64,64]{3,2,1,0:T(8,128)} copy(f32[16,8,64,64]{3,2,1,0:T(8,128)} %get-tuple-element.10) | data formatting | bytes 4194304
  (5 shorter events, 0.0 us)

commit v3 on v2

--- a/solution.py
+++ b/solution.py
@@ -24,7 +24,7 @@
 
 
 def device(z, g, c):
-    return (z, g // NX, g % NX, c)
+    return (z, g >> 2, g & 3, c)
 
 
 def remote(src, dst, send_sem, recv_sem, target):
@@ -57,6 +57,10 @@
     )
 
 
+def decay_of(head):
+    return 1.0 - jnp.exp2(-5.0 - 7.0 * head / (HEADS - 1))
+
+
 def row_scale(blocks):
     count = blocks.shape[0] * blocks.shape[2]
     total = jnp.sum(jnp.sum(blocks * blocks, axis=0), axis=-1, keepdims=True)
@@ -69,13 +73,13 @@
         self.send, self.recv = send, recv
 
     def out(self, i):
-        k = (self.me + i) % self.size
+        k = (self.me + i) & (self.size - 1)
         return remote(
             self.src(k), self.dst(self.me), self.send.at[k], self.recv.at[self.me], self.at(k)
         )
 
     def come(self, i):
-        k = (self.me + i) % self.size
+        k = (self.me + i) & (self.size - 1)
         return remote(
             self.src(k), self.dst(k), self.send.at[k], self.recv.at[k], self.at(k)
         )
@@ -91,14 +95,16 @@
 
 
 def layer_kernel(
-    tokens_ref, mix_ref, post_ref, ffn_ref, outg_ref, wsrc_ref, wot_ref, cos_ref, sin_ref, dec_ref, rt_ref,
+    tokens_ref, lengths_ref, mix_ref, post_ref, ffn_ref, outg_ref, wq_ref, wk_ref, wv_ref, wg_ref, wot_ref,
+    routes_ref, gates_ref, freq_ref,
     state_hbm, eg_hbm, eu_hbm, ed_hbm, sg_hbm, su_hbm, sd_hbm,
-    result_ref, new_hbm,
-    state, eg, eu, ed, sg, su, sd,
+    result_ref, state,
+    eg, eu, ed, sg, su, sd,
+    wsrc, packed, rt, trig,
     tbuf, abuf, wbuf, zbuf, wo, xsend, xbuf, osend, obuf, qbuf, onehot, comb_hi, comb_lo,
     kt, vsc, fs, rbuf, psend, pbuf, middle, mo, mbuf, shs, shb, ysend, ebuf, dsend, dbuf, ret, back,
     csend, cbuf, mixs, mixb,
-    l_s, w_s, a_s, a_r, t_s, t_r, b_s, b_r, c_s, c_r, d_s, d_r, q_s, q_r, o_s, o_r, r_s, r_r,
+    l_s, w_s, a_s, a_r, t_s, t_r, b_s, n_s, b_r, c_s, c_r, d_s, d_r, q_s, q_r, o_s, o_r, r_s, r_r,
     p_s, p_r, m_s, m_r, y_s, y_r, f_s, f_r, g_s, g_r, h_s, h_r, x_s, x_r,
 ):
     z, g, c = place()
@@ -111,22 +117,21 @@
     ]
     barrier = pltpu.get_barrier_semaphore()
 
-    def greet_plane(i):
-        other = (g * 2 + c + i) % (2 * NG)
+    for i in range(1, 2 * NG):
+        other = (g * 2 + c + i) & (2 * NG - 1)
         pl.semaphore_signal(
-            barrier, inc=1, device_id=device(z, other // 2, other % 2), device_id_type=MESH
-        )
-
-    def greet_column(i):
-        other = (z + 1 + i // 2) % NZ
-        pl.semaphore_signal(
-            barrier, inc=1, device_id=device(other, g, i % 2), device_id_type=MESH
-        )
-
-    each(1, 2 * NG, greet_plane)
-    each(0, 2 * NZ - 2, greet_column)
+            barrier, inc=1, device_id=device(z, other >> 1, other & 1), device_id_type=MESH
+        )
+    for i in range(1, NZ):
+        for core in range(2):
+            pl.semaphore_signal(
+                barrier, inc=1, device_id=device((z + i) & (NZ - 1), g, core), device_id_type=MESH
+            )
     for load in loads:
         load.start()
+    for m, w_ref in enumerate((wq_ref, wk_ref, wv_ref, wg_ref)):
+        for k in range(4):
+            wsrc[4 * m + k] = w_ref[:, k * 128 : (k + 1) * 128]
 
     half = tbuf.shape[-1]
     wide = tokens_ref[...].astype(F32)
@@ -134,6 +139,30 @@
     cols = pl.ds(pl.multiple_of(c * half, 128), half)
     part = tokens_ref[:, cols].astype(F32)
     tbuf[pl.ds(g, 1)] = (part * scale * mix_ref[:, cols]).astype(BF16)[None]
+    packed[...] = jnp.zeros_like(packed)
+    packed[0:6, 0:16] = routes_ref[...].astype(F32)
+    packed[8:14, 0:16] = gates_ref[...]
+    packed[14:15, 0:16] = lengths_ref[...].astype(F32)
+    turned = packed[...].T[0:16]
+    earlier = lax.broadcasted_iota(jnp.int32, (16, 16), 1) < lax.broadcasted_iota(
+        jnp.int32, (16, 16), 0
+    )
+    column_of = lax.broadcasted_iota(jnp.int32, (16, 16), 1)
+    table = turned
+    for k in range(6):
+        same = jnp.zeros((16, 16), F32)
+        for other in range(6):
+            same = jnp.where(
+                turned[:, k : k + 1] == packed[other : other + 1, 0:16], 1.0, same
+            )
+        rank = jnp.max(jnp.where(earlier, same, 0.0), axis=1, keepdims=True)
+        table = jnp.where(column_of == k, turned * 2.0 + rank, table)
+    rt[:, 0:16] = table
+    angles = turned[:, 14:15] * freq_ref[...]
+    first = lax.broadcasted_iota(jnp.int32, (16, 128), 1) % 64 < 32
+    trig[0] = jnp.cos(angles)
+    sines = jnp.sin(angles)
+    trig[1] = jnp.where(first, -sines, sines)
     pl.semaphore_wait(barrier, 2 * NG - 1 + 2 * NZ - 2)
 
     def plane(src, dst, send, recv):
@@ -142,48 +171,83 @@
     def column(src, dst, send, recv):
         return Group(z, NZ, lambda k: device(k, g, c), src, dst, send, recv)
 
-    ga = plane(lambda k: wsrc_ref.at[k], lambda k: abuf.at[k], a_s, a_r)
+    ga = plane(lambda k: wsrc.at[k], lambda k: abuf.at[k], a_s, a_r)
     gt = plane(lambda k: tbuf.at[g], lambda k: tbuf.at[k], t_s, t_r)
     gc = column(lambda k: wot_ref, lambda k: zbuf.at[k], c_s, c_r)
-    gq = column(lambda k: rt_ref, lambda k: qbuf.at[k], q_s, q_r)
+    gq = column(lambda k: rt, lambda k: qbuf.at[k], q_s, q_r)
     ga.start()
-    own_a = pltpu.make_async_copy(wsrc_ref.at[g], abuf.at[g], l_s.at[0])
+    own_a = pltpu.make_async_copy(wsrc.at[g], abuf.at[g], l_s.at[0])
     own_a.start()
-    gt.start()
     gc.start()
     gq.start()
     own_z = pltpu.make_async_copy(wot_ref, zbuf.at[z], l_s.at[1])
     own_z.start()
-    qbuf[pl.ds(z, 1)] = rt_ref[...][None]
+    qbuf[pl.ds(z, 1), :, 0:16] = rt[:, 0:16][None]
 
     ga.wait()
     own_a.wait()
-    b_core = z // (NZ // 2)
-
-    def b_copy(j):
-        other = (z + j) % NZ
+    b_core = z >> 2
+
+    def b_copy(n, delta):
         return remote(
-            abuf, wbuf.at[c, z % 4], b_s.at[j], b_r.at[c, z % 4], device(other, g, b_core)
-        )
-
-    each(1, NZ, lambda j: b_copy(j).start())
+            abuf,
+            wbuf.at[c, z & 3],
+            b_s.at[n],
+            b_r.at[c, z & 3],
+            device((z + delta) & (NZ - 1), g, b_core),
+        )
+
+    direct = ((0, 2), (1, -2), (2, 1), (3, -1))
+    for n, delta in direct:
+        b_copy(n, delta).start()
 
     @pl.when(b_core == c)
     def _():
-        pltpu.make_async_copy(abuf, wbuf.at[c, z % 4], b_r.at[c, z % 4]).start()
+        pltpu.make_async_copy(abuf, wbuf.at[c, z & 3], b_r.at[c, z & 3]).start()
 
     @pl.when(b_core != c)
     def _():
-        b_copy(0).start()
+        b_copy(4, 0).start()
+
+    gt.start()
+
+    def onward(delta, to, n, half_of):
+        source = (z + delta) & (NZ - 1)
+        block = wbuf.at[half_of, source & 3]
+        return remote(
+            block,
+            block,
+            n_s.at[half_of, n],
+            b_r.at[half_of, source & 3],
+            device((z + to) & (NZ - 1), g, c),
+        )
+
+    hops = ((-2, ((1, 0), (2, 1))), (2, ((-1, 2),)))
+
+    def forwards(act):
+        for delta, targets in hops:
+
+            @pl.when((((z + delta) & (NZ - 1)) >> 2) == c)
+            def _(delta=delta, targets=targets):
+                for half_of in range(2):
+                    act(delta, targets, half_of)
+
+    def pass_on(delta, targets, half_of):
+        source = (z + delta) & 3
+        pltpu.make_async_copy(
+            abuf, wbuf.at[half_of, source], b_r.at[half_of, source]
+        ).wait()
+        for to, n in targets:
+            onward(delta, to, n, half_of).start()
 
     gc.wait()
     own_z.wait()
-    to_half = g // (NG // 2)
+    to_half = g >> 3
 
     def d_copy(k):
         other = 2 * k + to_half
         return other, remote(
-            zbuf.at[k], wo.at[g % 8], d_s.at[k], d_r.at[g % 8], device(z, other, c)
+            zbuf.at[k], wo.at[(g & 7)], d_s.at[k], d_r.at[(g & 7)], device(z, other, c)
         )
 
     def d_start(k):
@@ -191,13 +255,14 @@
 
         @pl.when(other == g)
         def _():
-            pltpu.make_async_copy(zbuf.at[k], wo.at[g % 8], d_r.at[g % 8]).start()
+            pltpu.make_async_copy(zbuf.at[k], wo.at[(g & 7)], d_r.at[(g & 7)]).start()
 
         @pl.when(other != g)
         def _():
             copy.start()
 
     each(0, NZ, d_start)
+    forwards(pass_on)
 
     gq.wait()
     routing = qbuf[...].reshape(NZ * 16, 128)
@@ -220,7 +285,11 @@
     gt.wait()
 
     def b_wait(j):
-        pltpu.make_async_copy(abuf, wbuf.at[j // 4, j % 4], b_r.at[j // 4, j % 4]).wait()
+        source = c * 4 + (j & 3)
+
+        @pl.when(((source - z) & 3) != 2)
+        def _():
+            pltpu.make_async_copy(abuf, wbuf.at[j >> 2, j & 3], b_r.at[j >> 2, j & 3]).wait()
 
     each(0, NZ, b_wait)
     rows = NG * tbuf.shape[1]
@@ -238,16 +307,38 @@
     go = plane(lambda k: osend.at[k], lambda k: obuf.at[k], o_s, o_r)
     go.start()
     obuf[pl.ds(g, 1)] = osend[pl.ds(g, 1)]
+    for group in (ga, gt, gc, gq):
+        group.drain()
+    for n, delta in direct:
+        b_copy(n, delta).wait_send()
+
+    @pl.when(b_core != c)
+    def _():
+        b_copy(4, 0).wait_send()
+
+    def sent_on(delta, targets, half_of):
+        for to, n in targets:
+            onward(delta, to, n, half_of).wait_send()
+
+    forwards(sent_on)
+    swap.wait_send()
+
+    def d_sent(k):
+        other, copy = d_copy(k)
+
+        @pl.when(other != g)
+        def _():
+            copy.wait_send()
+
+    each(0, NZ, d_sent)
     loads[0].wait()
     fs[...] = jnp.zeros_like(fs)
     go.wait()
 
     low_half = lax.broadcasted_iota(jnp.int32, (16, 128), 1) < 64
-    first = lax.broadcasted_iota(jnp.int32, (16, 128), 1) % 64 < 32
-
     def rotate(v):
         other = jnp.where(first, pltpu.roll(v, 96, 1), pltpu.roll(v, 32, 1))
-        return v * cos_ref[...] + other * sin_ref[...]
+        return v * trig[0] + other * trig[1]
 
     def by_head(v):
         low = jnp.sum(jnp.where(low_half, v, 0.0), axis=-1, keepdims=True)
@@ -271,9 +362,7 @@
                 column_q = query_t[h * 64 : (h + 1) * 64, s : s + 1]
                 fs[h, s : s + 1, 0:64] = jnp.sum(column_q * held, axis=0, keepdims=True)
         from_state = jnp.where(low_half, fs[0], pltpu.roll(fs[1], 64, 1))
-        decay = jnp.where(
-            low_half[0:1], dec_ref[c, pl.ds(2 * hp, 1)], dec_ref[c, pl.ds(2 * hp + 1, 1)]
-        )
+        decay = decay_of((c * 8 + 2 * hp + jnp.where(low_half[0:1], 0, 1)).astype(F32))
         read = decay * from_state + by_head(query * key) * value
         read = read * lax.rsqrt(by_head(read * read) / HEAD + EPS)
         rbuf[pl.ds(g, 1), pl.ds(hp, 1)] = (read * jax.nn.silu(block(3))).astype(BF16)[None, None]
@@ -285,7 +374,7 @@
     def update_pair(hp):
         keys = kt[pl.ds(hp, 1)][0]
         for h in range(2):
-            decay = dec_ref[c, pl.ds(2 * hp + h, 1)][:, 0:64]
+            decay = decay_of(jnp.full((1, 64), c * 8 + 2 * hp + h, jnp.int32).astype(F32))
             value = vsc[pl.ds(2 * hp + h, 1)][0]
             for s in range(16):
                 held = state[s, pl.ds(2 * hp + h, 1)][0]
@@ -295,13 +384,11 @@
                 )[None]
 
     each(0, 4, update_pair)
-    store = pltpu.make_async_copy(state, new_hbm, w_s.at[7])
-    store.start()
-
     def d_wait(k):
         pltpu.make_async_copy(zbuf.at[k], wo.at[k], d_r.at[k]).wait()
 
     each(0, NZ, d_wait)
+    go.drain()
     gr.wait()
 
     partial = dot(wide_rows(rbuf[...]), wo[...].reshape(128, 512), ((1,), (1,)))
@@ -316,6 +403,7 @@
     )
     each(0, NG, lambda i: gp_other.out(i).start())
     pbuf[pl.ds(c, 1), pl.ds(g, 1)] = psend[pl.ds(g, 1)][None]
+    gr.drain()
     gp[0].wait()
     gp_from = Group(
         g, NG, lambda k: device(z, k, 1 - c), lambda k: psend.at[k], lambda k: pbuf.at[1 - c, k],
@@ -342,6 +430,8 @@
     shs[...] = parts.reshape(shs.shape)
     share = remote(shs.at[1 - c], shb, x_s.at[1], x_r.at[1], device(z, g, 1 - c))
     share.start()
+    gp[0].drain()
+    each(0, NG, lambda i: gp_other.out(i).wait_send())
     for load in loads[4:]:
         load.wait()
     gm.wait()
@@ -361,8 +451,9 @@
 
     def relay(i):
         gy.come(i).wait_recv()
-        forward(c, (g + i) % NG).start()
-
+        forward(c, (g + i) & (NG - 1)).start()
+
+    gm.drain()
     each(1, NG, relay)
 
     def expert_in(k):
@@ -392,6 +483,10 @@
     back[pl.ds(g, 1)] = ret[pl.ds(g, 1)]
     share.wait_recv()
     shared_out = (shs[pl.ds(c, 1)][0].astype(F32) + shb[...].astype(F32)).astype(BF16).astype(F32)
+    gy.drain()
+    each(0, NG, lambda k: forward(c, k).wait_send())
+    share.wait_send()
+    give.wait_send()
     gg.wait()
 
     answers = wide_rows(back[...])
@@ -401,6 +496,7 @@
     gh = column(lambda k: csend.at[k], lambda k: cbuf.at[k], h_s, h_r)
     gh.start()
     cbuf[pl.ds(z, 1)] = csend[pl.ds(z, 1)]
+    gg.drain()
     gh.wait()
     mixs[...] = shared_out + jnp.sum(cbuf[...].astype(F32), axis=0)
     last = remote(mixs, mixb, x_s.at[3], x_r.at[3], device(z, g, 1 - c))
@@ -413,33 +509,8 @@
     for k in range(NG):
         result_ref[:, k * 128 : (k + 1) * 128] = final[k]
 
-    for group in (ga, gt, gc, gq, go, gr, gp[0], gm, gy, gg, gh):
-        group.drain()
-    each(0, NG, lambda i: gp_other.out(i).wait_send())
-    each(1, NZ, lambda j: b_copy(j).wait_send())
-
-    @pl.when(b_core != c)
-    def _():
-        b_copy(0).wait_send()
-
-    def d_sent(k):
-        other, copy = d_copy(k)
-
-        @pl.when(other != g)
-        def _():
-            copy.wait_send()
-
-    each(0, NZ, d_sent)
-    each(0, NG, lambda k: forward(c, k).wait_send())
-    for copy in (swap, share, give, last):
-        copy.wait_send()
-    store.wait()
-
-
-def decay_table(head_count):
-    head_order = np.arange(head_count, dtype=np.float32)
-    decays = (1.0 - np.exp2(-5.0 - 7.0 * head_order / (head_count - 1))).astype(np.float32)
-    return np.broadcast_to(decays.reshape(2, -1, 1), (2, head_count // 2, 128))
+    gh.drain()
+    last.wait_send()
 
 
 def on_device(
@@ -448,20 +519,7 @@
     expert_gate, expert_up, expert_down, shared_gate, shared_up, shared_down,
 ):
     seq, width = tokens.shape
-    half_dim = HEAD // 2
-    frequency = THETA ** (-jnp.arange(half_dim, dtype=F32) / half_dim)
-    angles = lengths.astype(F32)[:, None] * frequency[None, :]
-    cosine, sine = jnp.cos(angles), jnp.sin(angles)
-    cos_table = jnp.concatenate([cosine] * 4, axis=1)
-    sin_table = jnp.concatenate([-sine, sine] * 2, axis=1)
-    earlier = jnp.arange(seq)[None, None, :, None] < jnp.arange(seq)[:, None, None, None]
-    same = routes[:, :, None, None] == routes[None, None]
-    rank = jnp.any(jnp.logical_and(same, earlier), axis=(2, 3)).astype(jnp.int32)
-    slot = (routes * 2 + rank).astype(F32)
-    gap = jnp.zeros((seq, 2), F32)
-    table = jnp.concatenate([slot, gap, route_gates, jnp.zeros((seq, 114), F32)], axis=1)
-    wsrc = jnp.concatenate((query_weight, key_weight, value_weight, gate_weight), axis=1)
-    wsrc = wsrc.reshape(seq, NG, 128).transpose(1, 0, 2)
+    frequency = THETA ** (-(np.arange(128) % 32).astype(np.float64) / 32)
     dma = pltpu.SemaphoreType.DMA
     blocks = pltpu.VMEM((NG, 16, 128), BF16)
     halves = pltpu.VMEM((NG, 8, 16, 128), BF16)
@@ -473,13 +531,17 @@
     return pl.pallas_call(
         layer_kernel,
         out_shape=(
-            jax.ShapeDtypeStruct((seq, width), BF16),
-            jax.ShapeDtypeStruct(prior_state.shape, F32),
+            pltpu.VMEM((seq, width), BF16),
+            pltpu.VMEM(prior_state.shape, F32),
         ),
-        in_specs=[vmem] * 11 + [anywhere] * 7,
-        out_specs=(vmem, anywhere),
+        in_specs=[vmem] * 14 + [anywhere] * 7,
+        out_specs=(vmem, vmem),
         scratch_shapes=[
-            *(pltpu.VMEM(array.shape, array.dtype) for array in big),
+            *(pltpu.VMEM(array.shape, array.dtype) for array in big[1:]),
+            blocks,
+            pltpu.VMEM((16, 128), F32),
+            pltpu.VMEM((16, 128), F32),
+            pltpu.VMEM((2, 16, 128), F32),
             pltpu.VMEM((NG, seq, width // 2), BF16),
             blocks,
             pltpu.VMEM((2, 4, NG, 16, 128), BF16),
@@ -518,7 +580,7 @@
             dma((8,)),
             plane_sems, plane_sems,
             plane_sems, plane_sems,
-            column_sems, dma((2, 4)),
+            dma((5,)), dma((2, 3)), dma((2, 4)),
             column_sems, column_sems,
             column_sems, column_sems,
             column_sems, column_sems,
@@ -532,18 +594,23 @@
             column_sems, column_sems,
             dma((4,)), dma((4,)),
         ],
-        compiler_params=pltpu.CompilerParams(collective_id=0, has_side_effects=True),
+        compiler_params=pltpu.CompilerParams(
+            collective_id=0, has_side_effects=True, vmem_limit_bytes=int(59.5 * 2**20)
+        ),
         name="layer",
     )(
         tokens,
+        lengths[None],
         mix_gain[None],
         *(gain.reshape(NG, 1, 128) for gain in (post_gain, ffn_gain, out_gain)),
-        wsrc,
+        query_weight,
+        key_weight,
+        value_weight,
+        gate_weight,
         out_weight.T,
-        cos_table,
-        sin_table,
-        jnp.asarray(decay_table(HEADS)),
-        table,
+        routes.T,
+        route_gates.T,
+        jnp.asarray(frequency[None], F32),
         *big,
     )
 

time: 111 us -> 93.9 us (0.85)
  local copies, waits for them, and re-layouts: 9.39 us -> 2.64 us
  Pallas kernels: 95.9 us -> 90.5 us
  other arithmetic: 4.61 us -> 0 us
    pallas_call x1, Pallas kernels: 95.9 us -> 90.5 us  [on_device(): pl.pallas_call(layer_kernel, out_shape=(pltpu.VMEM((seq, width), BF16), p...]
    unnamed x4 -> x2, local copies, waits for them, and re-layouts: 7.79 us -> 2.64 us
    transpose x1 -> x0, other arithmetic: 1.41 us -> none  [on_device(): wsrc = wsrc.reshape(seq, NG, 128).transpose(1, 0, 2)]
    concatenate x2 -> x0, other arithmetic: 1.36 us -> none  [the longest x1 0.69 us: on_device(): cos_table = jnp.concatenate([cosine] * 4, axis=1)]
    another operation x1 -> x0, local copies, waits for them, and re-layouts: 1.35 us -> none
where the time goes in v3:
time: 93.9 us; the launch traced here: 93.7 us
  Pallas kernels  90.5 us (96%)
  local copies, waits for them, and re-layouts  2.64 us (3%)
    pallas_call x1, Pallas kernels, on_device(): pl.pallas_call(layer_kernel, out_shape=(pltpu.VMEM((seq, width), BF16), p...  90.5 us
    unnamed x2, local copies, waits for them, and re-layouts  2.64 us

profile of v3, /device:TPU:1, one launch (start us, length us, event | category | flops | bytes accessed | tf_op | source)
XLA Modules:
  0.0 93.7 jit_solution(7309508453101598260)
XLA Ops:
  0.6 90.5 %layer.1 = (bf16[16,2048]{1,0:T(8,128)(2,1)S(1)}, f32[16,8,64,64]{3,2,1,0:T(8,128)S(1)}) custom-call(bf16[16,2048]{1,0:T(8,128)(2,1)} %tokens_ref.1, s32[1,16]{1,0:T(1,128)} %bitcast.15, f32[1,2048]{1,0:T(1,128)} %bitcast.9, f32[16,1,128]{2,1,0:T(1,128)} %bitcast.10, f32[16,1,128]{2,1,0:T(1,128)} %bitcast.11, f32[16,1,128]{2,1,0:T(1,128)} %bitcast.12, ...), custom_call_target="tpu_custom_call" | custom-call | tf_op jit(solution)/shard_map/layer/pallas_call | solution.py:531
  91.1 0.6 copy.25
  91.7 2.0 %copy.26 = f32[16,8,64,64]{3,2,1,0:T(8,128)} copy(f32[16,8,64,64]{3,2,1,0:T(8,128)S(1)} %get-tuple-element.3) | data formatting | bytes 4194304

commit v4 on v3

v4 whole, which is shorter than its diff:
```python
import jax
import jax.numpy as jnp
import numpy as np
from jax import lax
from jax.experimental import pallas as pl
from jax.experimental.pallas import tpu as pltpu
from jax.sharding import Mesh
from jax.sharding import PartitionSpec as P

HEAD = 64
HEADS = 16
EP = ("ep_0", "ep_1", "ep_2")
EPS = 1e-06
THETA = 10000.0
MESH = pl.DeviceIdType.MESH
NZ, NY, NX, NG = 8, 4, 4, 16
NCH = 4
PER = 8 // NCH
BF16 = jnp.bfloat16
F32 = jnp.float32


def place():
    z, y, x, c = (lax.axis_index(name) for name in ("ep_0", "ep_1", "ep_2", "tp"))
    return z, y * NX + x, c


def device(z, g, c):
    return (z, g >> 2, g & 3, c)


def remote(src, dst, send_sem, recv_sem, target):
    return pltpu.make_async_remote_copy(
        src_ref=src,
        dst_ref=dst,
        send_sem=send_sem,
        recv_sem=recv_sem,
        device_id=target,
        device_id_type=MESH,
    )


def each(low, high, body):
    def step(i, carry):
        body(i)
        return carry

    lax.fori_loop(low, high, step, 0)


def dot(a, b, dims=((1,), (0,))):
    return lax.dot_general(a, b, (dims, ((), ())), preferred_element_type=F32)


def wide_rows(blocks):
    rows = blocks.shape[0] * blocks.shape[2]
    return jnp.concatenate(
        [blocks[:, k].reshape(rows, 128) for k in range(blocks.shape[1])], axis=1
    )


def row_scale(blocks):
    count = blocks.shape[0] * blocks.shape[2]
    total = jnp.sum(jnp.sum(blocks * blocks, axis=0), axis=-1, keepdims=True)
    return lax.rsqrt(total / count + EPS)[None]


def arrived(blocks, sem):
    pltpu.make_async_copy(blocks, blocks, sem).wait()


class Exchange:
    def __init__(self, me, size, at, src, dst, send, recv):
        self.me, self.size, self.at, self.src, self.dst = me, size, at, src, dst
        self.send, self.recv = send, recv

    def out(self, i):
        k = (self.me + i) & (self.size - 1)
        return remote(self.src(k), self.dst(self.me), self.send, self.recv, self.at(k))

    def start(self, first=1):
        each(first, self.size, lambda i: self.out(i).start())


def layer_kernel(
    tokens_hbm, routes_hbm, gates_hbm, lengths_hbm, freq_hbm, mix_hbm, wot_hbm, post_hbm, ffn_hbm, outg_hbm,
    wq_hbm, wk_hbm, wv_hbm, wg_hbm,
    state_hbm, eg_hbm, eu_hbm, ed_hbm, sg_hbm, su_hbm, sd_hbm,
    result_ref, new_hbm,
    state,
    tokens_ref, routes_ref, gates_ref, lengths_ref, freq_ref, mix_ref, wot_ref, post_ref, ffn_ref, outg_ref,
    eg, eu, ed, sg, su, sd,
    wsrc, packed, rt, trig,
    tbuf, abuf, wbuf, zbuf, wo, osend, obuf, qbuf, onehot, comb_hi, comb_lo,
    qt, kt, vsc, fs, decays, rbuf, psend, pbuf, middle, mo, mbuf, shs, shb, ysend, ebuf, dsend, dbuf, ret, back,
    csend, cbuf, mixs, mixb,
    i_s, v_s, w_s, a_s, a_r, t_s, t_r, u_s, u_r, b_s, n_s, b_r, c_s, c_r, d_s, d_r, q_s, q_r,
    o_s, o_r, r_s, r_r, p_s, p_r, m_s, m_r, y_s, y_r, f_s, f_r, e_s, e_r, g_s, g_r, h_s, h_r, x_s, x_r,
):
    z, g, c = place()
    loads = [
        pltpu.make_async_copy(src, dst, w_s.at[i])
        for i, (src, dst) in enumerate(
            ((state_hbm, state), (sg_hbm, sg), (su_hbm, su), (sd_hbm, sd),
             (eg_hbm, eg), (eu_hbm, eu), (ed_hbm, ed))
        )
    ]
    barrier = pltpu.get_barrier_semaphore()

    for i in range(1, 2 * NG):
        other = (g * 2 + c + i) & (2 * NG - 1)
        pl.semaphore_signal(
            barrier, inc=1, device_id=device(z, other >> 1, other & 1), device_id_type=MESH
        )
    for i in range(1, NZ):
        for core in range(2):
            pl.semaphore_signal(
                barrier, inc=1, device_id=device((z + i) & (NZ - 1), g, core), device_id_type=MESH
            )
    small = [
        pltpu.make_async_copy(src, dst, i_s.at[i])
        for i, (src, dst) in enumerate(
            ((tokens_hbm, tokens_ref), (mix_hbm, mix_ref), (routes_hbm, routes_ref),
             (gates_hbm, gates_ref), (lengths_hbm, lengths_ref), (freq_hbm, freq_ref),
             (wot_hbm, wot_ref), (post_hbm, post_ref), (ffn_hbm, ffn_ref), (outg_hbm, outg_ref))
        )
    ]
    slices = [
        pltpu.make_async_copy(
            w_ref.at[:, pl.ds(k * 128, 128)], wsrc.at[4 * m + k], v_s
        )
        for m, w_ref in enumerate((wq_hbm, wk_hbm, wv_hbm, wg_hbm))
        for k in range(4)
    ]
    for load in small[:2] + slices + small[2:] + loads:
        load.start()
    for load in small[:6]:
        load.wait()
    half = tbuf.shape[-1]
    wide = tokens_ref[...].astype(F32)
    scale = lax.rsqrt(jnp.mean(wide * wide, axis=-1, keepdims=True) + EPS)
    normed = (wide * scale * mix_ref[...]).astype(BF16)
    for k in range(2):
        tbuf[k, pl.ds(g, 1)] = normed[:, k * half : (k + 1) * half][None]
    packed[...] = jnp.zeros_like(packed)
    packed[0:6, 0:16] = routes_ref[...].astype(F32)
    packed[8:14, 0:16] = gates_ref[...]
    packed[14:15, 0:16] = lengths_ref[...].astype(F32)
    turned = packed[...].T[0:16]
    earlier = lax.broadcasted_iota(jnp.int32, (16, 16), 1) < lax.broadcasted_iota(
        jnp.int32, (16, 16), 0
    )
    column_of = lax.broadcasted_iota(jnp.int32, (16, 16), 1)
    table = turned
    for k in range(6):
        same = jnp.zeros((16, 16), F32)
        for other in range(6):
            same = jnp.where(
                turned[:, k : k + 1] == packed[other : other + 1, 0:16], 1.0, same
            )
        rank = jnp.max(jnp.where(earlier, same, 0.0), axis=1, keepdims=True)
        table = jnp.where(column_of == k, turned * 2.0 + rank, table)
    rt[:, 0:16] = table
    for load in small[6:]:
        load.wait()
    arrived(wsrc, v_s)
    pl.semaphore_wait(barrier, 2 * NG - 1 + 2 * NZ - 2)

    def plane(src, dst, send, recv):
        return Exchange(g, NG, lambda k: device(z, k, c), src, dst, send, recv)

    def column(src, dst, send, recv):
        return Exchange(z, NZ, lambda k: device(k, g, c), src, dst, send, recv)

    others, above = pl.ds(0, NG - 1), pl.ds(0, NZ - 1)

    ga = plane(lambda k: wsrc.at[k], lambda k: abuf.at[k], a_s, a_r)
    gt = plane(lambda k: tbuf.at[c, g], lambda k: tbuf.at[c, k], t_s, t_r.at[g])
    gc = column(lambda k: wot_ref, lambda k: zbuf.at[k], c_s, c_r)
    gq = column(lambda k: rt, lambda k: qbuf.at[k], q_s, q_r)
    ga.start()
    pltpu.make_async_copy(wsrc.at[g], abuf.at[g], a_r).start()
    gq.start()
    qbuf[pl.ds(z, 1), :, 0:16] = rt[:, 0:16][None]

    arrived(abuf, a_r)

    def b_copy(delta):
        return remote(
            abuf, wbuf.at[z], b_s, b_r.at[z], device((z + delta) & (NZ - 1), g, c)
        )

    for delta in (2, -2, 1, -1):
        b_copy(delta).start()
    pltpu.make_async_copy(abuf, wbuf.at[z], b_r.at[z]).start()
    gt.start()

    def b_wait(delta):
        source = (z + delta) & (NZ - 1)
        pltpu.make_async_copy(abuf, wbuf.at[source], b_r.at[source]).wait()

    def onward(delta, to):
        source = (z + delta) & (NZ - 1)
        return remote(
            wbuf.at[source],
            wbuf.at[source],
            n_s,
            b_r.at[source],
            device((z + to) & (NZ - 1), g, c),
        )

    to_half = g >> 3

    def d_start(k):
        other = 2 * k + to_half

        @pl.when(other == g)
        def _():
            pltpu.make_async_copy(zbuf.at[k], wo.at[g & 7], d_r).start()

        @pl.when(other != g)
        def _():
            remote(zbuf.at[k], wo.at[g & 7], d_s, d_r, device(z, other, c)).start()

    arrived(qbuf.at[above], q_r)
    routing = qbuf[...].reshape(NZ * 16, 128)
    slots = 16 * NG
    row_z = lax.broadcasted_iota(jnp.int32, (NZ * 16, slots), 0) // 16
    lane = lax.broadcasted_iota(jnp.int32, (NZ * 16, slots), 1)
    slot_id = ((z * NG + lane // 16) * 2 + lane % 2).astype(F32)
    same_z = row_z == (lane % 16) // 2
    named = jnp.zeros((NZ * 16, slots), F32)
    weight = jnp.zeros((NZ * 16, slots), F32)
    for k in range(6):
        hit = jnp.logical_and(routing[:, k : k + 1] == slot_id, same_z)
        named = named + jnp.where(hit, 1.0, 0.0)
        weight = weight + jnp.where(hit, routing[:, 8 + k : 9 + k], 0.0)
    onehot[...] = named.T.astype(BF16)
    upper = weight.astype(BF16)
    comb_hi[...] = upper
    comb_lo[...] = (weight - upper.astype(F32)).astype(BF16)

    angles = rt[:, 14:15] * freq_ref[...]
    first = lax.broadcasted_iota(jnp.int32, (16, 128), 1) % 64 < 32
    trig[0] = jnp.cos(angles)
    sines = jnp.sin(angles)
    trig[1] = jnp.where(first, -sines, sines)
    heads = lax.broadcasted_iota(jnp.int32, (8, 128), 0) + c * 8
    decays[...] = 1.0 - jnp.exp2(-5.0 - 7.0 * heads.astype(F32) / (HEADS - 1))
    b_wait(-2)
    onward(-2, 2).start()
    onward(-2, 1).start()
    b_wait(2)
    onward(2, -1).start()

    def t_forward(half_of, k):
        block = tbuf.at[half_of, k]
        return remote(block, block, u_s, u_r, device(z, g, 1 - c))

    def t_relay(i):
        k = (g + i) & (NG - 1)
        arrived(tbuf.at[c, k], t_r.at[k])
        t_forward(c, k).start()

    each(1, NG, t_relay)
    arrived(tbuf.at[1 - c, others], u_r)

    for delta in (0, 1, -1, 3, -3, 4):
        b_wait(delta)
    rows = NG * tbuf.shape[2]
    mine = dot(tbuf[0].reshape(rows, half), wbuf[0:4].reshape(half, 128)) + dot(
        tbuf[1].reshape(rows, half), wbuf[4:8].reshape(half, 128)
    )
    osend[...] = mine.astype(BF16).reshape(osend.shape)
    go = plane(lambda k: osend.at[k], lambda k: obuf.at[k], o_s, o_r)
    go.start()
    gc = column(lambda k: wot_ref, lambda k: zbuf.at[z], c_s, c_r)
    gc.start()
    pltpu.make_async_copy(wot_ref, zbuf.at[z], c_r).start()
    obuf[pl.ds(g, 1)] = osend[pl.ds(g, 1)]
    arrived(abuf.at[others], a_s)
    arrived(tbuf.at[c, others], t_s)
    arrived(tbuf.at[c, others], u_s)
    arrived(qbuf.at[above], q_s)
    arrived(wbuf.at[pl.ds(0, 4)], b_s)
    arrived(wbuf.at[pl.ds(0, 3)], n_s)
    loads[0].wait()
    arrived(obuf.at[others], o_r)
    arrived(zbuf, c_r)
    each(0, NZ, d_start)
    low_half = lax.broadcasted_iota(jnp.int32, (16, 128), 1) < 64
    def rotate(v):
        other = jnp.where(first, pltpu.roll(v, 96, 1), pltpu.roll(v, 32, 1))
        return v * trig[0] + other * trig[1]

    def by_head(v):
        low = jnp.sum(jnp.where(low_half, v, 0.0), axis=-1, keepdims=True)
        high = jnp.sum(jnp.where(low_half, 0.0, v), axis=-1, keepdims=True)
        return jnp.where(low_half, low, high)

    def block(k, hp):
        return obuf[4 * k + hp].astype(F32)

    self_terms = []
    for hp in range(4):
        query = rotate(block(0, hp))
        key = rotate(block(1, hp)) * HEAD ** (-0.5)
        value = block(2, hp)
        qt[hp] = query.T
        kt[hp] = key.T
        vsc[2 * hp] = value
        vsc[2 * hp + 1] = pltpu.roll(value, 64, 1)
        self_terms.append(by_head(query * key) * value)

    def read_pair(hp):
        queries = qt[pl.ds(hp, 1)][0]
        for h in range(2):
            for s in range(16):
                held = state[s, pl.ds(2 * hp + h, 1)][0]
                column_q = queries[h * 64 : (h + 1) * 64, s : s + 1]
                fs[pl.ds(2 * hp + h, 1), s : s + 1, 0:64] = jnp.sum(
                    column_q * held, axis=0, keepdims=True
                )[None]

    each(0, 4, read_pair)
    for hp in range(4):
        from_state = jnp.where(low_half, fs[2 * hp], pltpu.roll(fs[2 * hp + 1], 64, 1))
        decay = jnp.where(
            low_half[0:1], decays[2 * hp : 2 * hp + 1], decays[2 * hp + 1 : 2 * hp + 2]
        )
        read = decay * from_state + self_terms[hp]
        read = read * lax.rsqrt(by_head(read * read) / HEAD + EPS)
        rbuf[pl.ds(g, 1), hp] = (read * jax.nn.silu(block(3, hp))).astype(BF16)[None]
    gr = plane(lambda k: rbuf.at[g], lambda k: rbuf.at[g], r_s, r_r)
    gr.start()

    def update_pair(hp):
        keys = kt[pl.ds(hp, 1)][0]
        for h in range(2):
            decay = decays[pl.ds(2 * hp + h, 1), 0:64]
            value = vsc[pl.ds(2 * hp + h, 1)][0]
            for s in range(16):
                held = state[s, pl.ds(2 * hp + h, 1)][0]
                column_k = keys[h * 64 : (h + 1) * 64, s : s + 1]
                state[s, pl.ds(2 * hp + h, 1)] = (
                    decay * held + column_k * value[s : s + 1, 0:64]
                )[None]

    each(0, 4, update_pair)
    def d_wait(k):
        pltpu.make_async_copy(zbuf.at[k], wo.at[k], d_r.at[k]).wait()

    store = pltpu.make_async_copy(state, new_hbm, w_s.at[7])
    store.start()
    arrived(obuf.at[others], o_s)
    arrived(zbuf.at[above], c_s)

    @pl.when((g & 1) == to_half)
    def _():
        arrived(zbuf.at[above], d_s)

    @pl.when((g & 1) != to_half)
    def _():
        arrived(zbuf, d_s)

    arrived(wo, d_r)
    arrived(rbuf.at[others], r_r)
    partial = dot(wide_rows(rbuf[...]), wo[...].reshape(128, 512), ((1,), (1,)))
    psend[...] = partial.astype(BF16).reshape(psend.shape)
    gp = plane(lambda k: psend.at[k], lambda k: pbuf.at[c, k], p_s.at[0], p_r.at[0])
    gp.start()
    gp_other = Exchange(
        g, NG, lambda k: device(z, k, 1 - c), lambda k: psend.at[k], lambda k: pbuf.at[c, k],
        p_s.at[1], p_r.at[1],
    )
    gp_other.start(0)
    pbuf[pl.ds(c, 1), pl.ds(g, 1)] = psend[pl.ds(g, 1)][None]
    arrived(rbuf.at[others], r_s)
    arrived(psend.at[others], p_r.at[0])
    arrived(psend, p_r.at[1])
    mixed = (pbuf[0].astype(F32) + pbuf[1].astype(F32)).astype(BF16).astype(F32)
    tok = jnp.stack([tokens_ref[:, k * 128 : (k + 1) * 128] for k in range(NG)]).astype(F32)
    mid = (tok + mixed * row_scale(mixed) * post_ref[...]).astype(BF16)
    middle[...] = mid
    mid = mid.astype(F32)
    mo[...] = (mid * row_scale(mid) * ffn_ref[...]).astype(BF16)

    for n in range(NCH):
        blocks = pl.ds(c * 8 + n * PER, PER)
        mbuf[n, pl.ds(z, 1)] = mo[blocks][None]
        gm = column(lambda k, n=n: mbuf.at[n, z], lambda k, n=n: mbuf.at[n, k], m_s, m_r.at[n])
        gm.start()
    for load in loads[1:4]:
        load.wait()
    rows_in = wide_rows(mo[...][None])
    shared_hidden = (jax.nn.silu(dot(rows_in, sg[...])) * dot(rows_in, su[...])).astype(BF16)
    shared_part = dot(shared_hidden, sd[...]).astype(BF16)
    parts = jnp.stack([shared_part[:, k * 128 : (k + 1) * 128] for k in range(NG)])
    shs[...] = parts.reshape(shs.shape)
    share = remote(shs.at[1 - c], shb, x_s.at[0], x_r.at[0], device(z, g, 1 - c))
    share.start()
    for load in loads[4:]:
        load.wait()
    arrived(psend.at[others], p_s.at[0])
    arrived(psend, p_s.at[1])
    for n in range(NCH):
        arrived(mbuf.at[n, above], m_r.at[n])
        sorted_rows = dot(onehot[...], wide_rows(mbuf[n])).astype(BF16)
        for k in range(PER):
            ysend[n, :, k] = sorted_rows[:, k * 128 : (k + 1) * 128].reshape(NG, 16, 128)
        gy = plane(lambda k, n=n: ysend.at[n, k], lambda k, n=n: ebuf.at[n, c, k], y_s, y_r.at[n])
        gy.start()
        ebuf[n, pl.ds(c, 1), pl.ds(g, 1)] = ysend[n, pl.ds(g, 1)][None]
    arrived(mbuf.at[:, above], m_s)

    def forward(n):
        rows = ebuf.at[n, c]
        return remote(rows, rows, f_s.at[n], f_r.at[n], device(z, g, 1 - c))

    def expert_in(n, k):
        blocks = wide_rows(ebuf[n, pl.ds(k, 1)][0])
        rows_of = pl.ds(pl.multiple_of(k * half + n * PER * 128, 128), PER * 128)
        return dot(blocks, eg[0, rows_of]), dot(blocks, eu[0, rows_of])

    gates, ups = [], []
    for n in range(NCH):
        arrived(ebuf.at[n, c, others], y_r.at[n])
        forward(n).start()
        gate, up = expert_in(n, c)
        gates.append(gate)
        ups.append(up)
    for n in range(NCH):
        arrived(ebuf.at[n, 1 - c], f_r.at[n])
        gate, up = expert_in(n, 1 - c)
        gates.append(gate)
        ups.append(up)
    hidden = (jax.nn.silu(sum(gates)) * sum(ups)).astype(BF16)

    def down(n, k):
        cols_of = pl.ds(pl.multiple_of(k * half + n * PER * 128, 128), PER * 128)
        out = dot(hidden, ed[0, :, cols_of]).astype(BF16)
        return [out[:, j * 128 : (j + 1) * 128].reshape(NG, 16, 128) for j in range(PER)]

    def give(n):
        return remote(dsend.at[n], dbuf.at[n], e_s.at[n], e_r.at[n], device(z, g, 1 - c))

    for n in range(NCH):
        for j, rows in enumerate(down(n, 1 - c)):
            dsend[n, :, j] = rows
        give(n).start()
    for n in range(NCH):
        kept = down(n, c)
        give(n).wait_recv()
        for j in range(PER):
            ret[n, :, j] = (kept[j].astype(F32) + dbuf[n, :, j].astype(F32)).astype(BF16)
        gg = plane(lambda k, n=n: ret.at[n, k], lambda k, n=n: back.at[n, k], g_s, g_r.at[n])
        gg.start()
        back[n, pl.ds(g, 1)] = ret[n, pl.ds(g, 1)]
    share.wait_recv()
    shared_out = (shs[pl.ds(c, 1)][0].astype(F32) + shb[...].astype(F32)).astype(BF16).astype(F32)
    arrived(ysend.at[:, others], y_s)
    for n in range(NCH):
        forward(n).wait_send()
        give(n).wait_send()
    share.wait_send()

    for n in range(NCH):
        arrived(back.at[n, others], g_r.at[n])
        answers = wide_rows(back[n])
        sums = (dot(comb_hi[...], answers) + dot(comb_lo[...], answers)).astype(BF16)
        for k in range(PER):
            csend[n, :, k] = sums[:, k * 128 : (k + 1) * 128].reshape(NZ, 16, 128)
        gh = column(lambda k, n=n: csend.at[n, k], lambda k, n=n: cbuf.at[n, k], h_s, h_r.at[n])
        gh.start()
        cbuf[n, pl.ds(z, 1)] = csend[n, pl.ds(z, 1)]
    arrived(ret.at[:, others], g_s)
    for n in range(NCH):
        arrived(cbuf.at[n, above], h_r.at[n])
        part = slice(n * PER, (n + 1) * PER)
        mixs[part] = shared_out[part] + jnp.sum(cbuf[n].astype(F32), axis=0)
    last = remote(mixs, mixb, x_s.at[1], x_r.at[1], device(z, g, 1 - c))
    last.start()
    last.wait_recv()
    first_half = jnp.where(c == 0, mixs[...], mixb[...])
    second_half = jnp.where(c == 0, mixb[...], mixs[...])
    mixture = jnp.concatenate([first_half, second_half], axis=0)
    final = (middle[...].astype(F32) + mixture * row_scale(mixture) * outg_ref[...]).astype(BF16)
    for k in range(NG):
        result_ref[:, k * 128 : (k + 1) * 128] = final[k]
    arrived(csend.at[:, above], h_s)
    last.wait_send()
    store.wait()


def on_device(
    tokens, lengths, prior_state, mix_gain, post_gain, ffn_gain, out_gain,
    query_weight, key_weight, value_weight, gate_weight, out_weight, routes, route_gates,
    expert_gate, expert_up, expert_down, shared_gate, shared_up, shared_down,
):
    seq, width = tokens.shape
    frequency = THETA ** (-(np.arange(128) % 32).astype(np.float64) / 32)
    dma = pltpu.SemaphoreType.DMA
    blocks = pltpu.VMEM((NG, 16, 128), BF16)
    halves = pltpu.VMEM((NCH, NG, PER, 16, 128), BF16)
    columns_of = pltpu.VMEM((NCH, NZ, PER, 16, 128), BF16)
    vmem = pl.BlockSpec(memory_space=pltpu.VMEM)
    anywhere = pl.BlockSpec(memory_space=pl.ANY)
    big = (prior_state, expert_gate, expert_up, expert_down, shared_gate, shared_up, shared_down)
    chunk_sems = dma((NCH,))
    post, ffn, outer = (gain.reshape(NG, 1, 128) for gain in (post_gain, ffn_gain, out_gain))
    small = (
        tokens, routes.T, route_gates.T, lengths[None], jnp.asarray(frequency[None], F32),
        mix_gain[None], out_weight.T, post, ffn, outer,
    )
    columns = (query_weight, key_weight, value_weight, gate_weight)
    return pl.pallas_call(
        layer_kernel,
        out_shape=(
            pltpu.VMEM((seq, width), BF16),
            pltpu.VMEM(prior_state.shape, F32),
        ),
        in_specs=[anywhere] * (len(small) + len(columns) + len(big)),
        out_specs=(vmem, anywhere),
        scratch_shapes=[
            pltpu.VMEM(prior_state.shape, F32),
            *(pltpu.VMEM(array.shape, array.dtype) for array in small + big[1:]),
            blocks,
            pltpu.VMEM((16, 128), F32),
            pltpu.VMEM((16, 128), F32),
            pltpu.VMEM((2, 16, 128), F32),
            pltpu.VMEM((2, NG, seq, width // 2), BF16),
            blocks,
            pltpu.VMEM((NZ, NG, 16, 128), BF16),
            pltpu.VMEM((8, 16, 512), BF16),
            pltpu.VMEM((8, 16, 512), BF16),
            blocks,
            blocks,
            pltpu.VMEM((NZ, 16, 128), F32),
            pltpu.VMEM((16 * NG, 16 * NZ), BF16),
            pltpu.VMEM((16 * NZ, 16 * NG), BF16),
            pltpu.VMEM((16 * NZ, 16 * NG), BF16),
            pltpu.VMEM((4, 128, 16), F32),
            pltpu.VMEM((4, 128, 16), F32),
            pltpu.VMEM((8, 16, 128), F32),
            pltpu.VMEM((8, 16, 128), F32),
            pltpu.VMEM((8, 128), F32),
            pltpu.VMEM((NG, 4, 16, 128), BF16),
            blocks,
            pltpu.VMEM((2, NG, 16, 128), BF16),
            blocks,
            blocks,
            columns_of,
            pltpu.VMEM((2, 8, 16, 128), BF16),
            pltpu.VMEM((8, 16, 128), BF16),
            halves,
            pltpu.VMEM((NCH, 2, NG, PER, 16, 128), BF16),
            halves,
            halves,
            halves,
            halves,
            columns_of,
            columns_of,
            pltpu.VMEM((8, 16, 128), F32),
            pltpu.VMEM((8, 16, 128), F32),
            dma((len(small),)),
            dma,
            dma((8,)),
            dma, dma,
            dma, dma((NG,)),
            dma, dma,
            dma, dma, dma((NZ,)),
            dma, dma, dma, dma, dma, dma,
            dma, dma, dma, dma,
            dma((2,)), dma((2,)),
            dma, chunk_sems,
            dma, chunk_sems,
            chunk_sems, chunk_sems,
            chunk_sems, chunk_sems,
            dma, chunk_sems,
            dma, chunk_sems,
            dma((2,)), dma((2,)),
        ],
        compiler_params=pltpu.CompilerParams(
            collective_id=0, has_side_effects=True, vmem_limit_bytes=int(59.5 * 2**20)
        ),
        name="layer",
    )(
        *small,
        *columns,
        *big,
    )


def solution(mesh):
    finer = Mesh(mesh.devices.reshape(8, 4, 4, mesh.shape["tp"]), ("ep_0", "ep_1", "ep_2", "tp"))
    in_specs = (
        P(EP, None),
        P(EP),
        P(EP, "tp", None, None),
        P(),
        P(),
        P(),
        P(),
        P(EP, "tp"),
        P(EP, "tp"),
        P(EP, "tp"),
        P(EP, "tp"),
        P("tp", EP),
        P(EP, None),
        P(EP, None),
        P(EP, None, "tp"),
        P(EP, None, "tp"),
        P(EP, "tp", None),
        P(None, "tp"),
        P(None, "tp"),
        P("tp", None),
    )
    out_specs = (P(EP, None), P(EP, "tp", None, None))
    return jax.shard_map(
        on_device, mesh=finer, in_specs=in_specs, out_specs=out_specs, check_vma=False
    )
```

time: 93.9 us -> 84.6 us (0.901)
  Pallas kernels: 90.5 us -> 81.3 us
    pallas_call x1, Pallas kernels: 90.5 us -> 81.3 us  [on_device(): pl.pallas_call(layer_kernel, out_shape=(pltpu.VMEM((seq, width), BF16), p...]
where the time goes in v4:
time: 84.6 us
  Pallas kernels  81.3 us (96%)
  local copies, waits for them, and re-layouts  2.64 us (3%)
    pallas_call x1, Pallas kernels, on_device(): pl.pallas_call(layer_kernel, out_shape=(pltpu.VMEM((seq, width), BF16), p...  81.3 us
    unnamed x2, local copies, waits for them, and re-layouts  2.64 us

profile of v4, /device:TPU:1, one launch (start us, length us, event | category | flops | bytes accessed | tf_op | source)
XLA Modules:
  0.0 84.6 jit_solution(16679115321245253009)
XLA Ops:
  0.6 81.3 %layer.1 = (bf16[16,2048]{1,0:T(8,128)(2,1)S(1)}, f32[16,8,64,64]{3,2,1,0:T(8,128)S(1)}) custom-call(bf16[16,2048]{1,0:T(8,128)(2,1)} %tokens_hbm.1, s32[6,16]{1,0:T(8,128)} %bitcast.13, f32[6,16]{1,0:T(8,128)} %bitcast.14, s32[1,16]{1,0:T(1,128)} %bitcast.15, f32[1,128]{1,0:T(1,128)} %constant.2.clone.freq_hbm, f32[1,2048]{1,0:T(1,128)} %bitcast.9, ...), custom_call_target="tpu_custom_call" | custom-call | tf_op jit(solution)/shard_map/layer/pallas_call | solution.py:516
  81.9 0.6 copy.25
  82.5 2.0 %copy.26 = f32[16,8,64,64]{3,2,1,0:T(8,128)} copy(f32[16,8,64,64]{3,2,1,0:T(8,128)S(1)} %get-tuple-element.3) | data formatting | bytes 4194304

commit v5 on v4

--- a/solution.py
+++ b/solution.py
@@ -16,6 +16,12 @@
 NZ, NY, NX, NG = 8, 4, 4, 16
 NCH = 4
 PER = 8 // NCH
+FAR_FIRST = {
+    NZ: sorted(range(NZ), key=lambda step: -min(step, NZ - step)),
+    NG: sorted(
+        range(NG), key=lambda step: -min(step // 4, 4 - step // 4) - min(step % 4, 4 - step % 4)
+    ),
+}
 BF16 = jnp.bfloat16
 F32 = jnp.float32
 
@@ -69,17 +75,25 @@
     pltpu.make_async_copy(blocks, blocks, sem).wait()
 
 
+def in_turn(me, size, step):
+    if size == NG:
+        return ((me + 4 * (step // 4)) & 12) + ((me + step % 4) & 3)
+    return (me + step) & (size - 1)
+
+
 class Exchange:
     def __init__(self, me, size, at, src, dst, send, recv):
         self.me, self.size, self.at, self.src, self.dst = me, size, at, src, dst
         self.send, self.recv = send, recv
 
-    def out(self, i):
-        k = (self.me + i) & (self.size - 1)
+    def out(self, step):
+        k = in_turn(self.me, self.size, step)
         return remote(self.src(k), self.dst(self.me), self.send, self.recv, self.at(k))
 
     def start(self, first=1):
-        each(first, self.size, lambda i: self.out(i).start())
+        for step in FAR_FIRST[self.size]:
+            if step >= first:
+                self.out(step).start()
 
 
 def layer_kernel(
@@ -92,31 +106,32 @@
     eg, eu, ed, sg, su, sd,
     wsrc, packed, rt, trig,
     tbuf, abuf, wbuf, zbuf, wo, osend, obuf, qbuf, onehot, comb_hi, comb_lo,
-    qt, kt, vsc, fs, decays, rbuf, psend, pbuf, middle, mo, mbuf, shs, shb, ysend, ebuf, dsend, dbuf, ret, back,
-    csend, cbuf, mixs, mixb,
+    qt, kt, vsc, fs, decays, rbuf, psend, pbuf, middle, mo, mbuf, shs, shb, ysend, ebuf, ret, back,
+    csend, cbuf, mixs, mixb, hid,
     i_s, v_s, w_s, a_s, a_r, t_s, t_r, u_s, u_r, b_s, n_s, b_r, c_s, c_r, d_s, d_r, q_s, q_r,
-    o_s, o_r, r_s, r_r, p_s, p_r, m_s, m_r, y_s, y_r, f_s, f_r, e_s, e_r, g_s, g_r, h_s, h_r, x_s, x_r,
+    o_s, o_r, r_s, r_r, p_s, p_r, m_s, m_r, y_s, y_r, f_s, f_r, g_s, g_r, h_s, h_r, x_s, x_r,
 ):
     z, g, c = place()
     loads = [
         pltpu.make_async_copy(src, dst, w_s.at[i])
         for i, (src, dst) in enumerate(
             ((state_hbm, state), (sg_hbm, sg), (su_hbm, su), (sd_hbm, sd),
-             (eg_hbm, eg), (eu_hbm, eu), (ed_hbm, ed))
+             (eg_hbm, eg), (eu_hbm, eu), (ed_hbm.at[0, :, pl.ds(pl.multiple_of(c * 1024, 128), 1024)], ed.at[c]))
         )
     ]
     barrier = pltpu.get_barrier_semaphore()
 
-    for i in range(1, 2 * NG):
-        other = (g * 2 + c + i) & (2 * NG - 1)
-        pl.semaphore_signal(
-            barrier, inc=1, device_id=device(z, other >> 1, other & 1), device_id_type=MESH
-        )
-    for i in range(1, NZ):
+    def greet(target):
+        pl.semaphore_signal(barrier, inc=1, device_id=target, device_id_type=MESH)
+
+    for step in FAR_FIRST[NZ][:-1]:
         for core in range(2):
-            pl.semaphore_signal(
-                barrier, inc=1, device_id=device((z + i) & (NZ - 1), g, core), device_id_type=MESH
-            )
+            greet(device((z + step) & (NZ - 1), g, core))
+    for step in FAR_FIRST[NG]:
+        k = in_turn(g, NG, step)
+        if step:
+            greet(device(z, k, c))
+        greet(device(z, k, 1 - c))
     small = [
         pltpu.make_async_copy(src, dst, i_s.at[i])
         for i, (src, dst) in enumerate(
@@ -132,8 +147,25 @@
         for m, w_ref in enumerate((wq_hbm, wk_hbm, wv_hbm, wg_hbm))
         for k in range(4)
     ]
-    for load in small[:2] + slices + small[2:] + loads:
+    for load in slices + small:
         load.start()
+    arrived(wsrc, v_s)
+    pl.semaphore_wait(barrier, 2 * NG - 1 + 2 * NZ - 2)
+
+    def plane(src, dst, send, recv):
+        return Exchange(g, NG, lambda k: device(z, k, c), src, dst, send, recv)
+
+    def column(src, dst, send, recv):
+        return Exchange(z, NZ, lambda k: device(k, g, c), src, dst, send, recv)
+
+    others, above = pl.ds(0, NG - 1), pl.ds(0, NZ - 1)
+
+    ga = plane(lambda k: wsrc.at[k], lambda k: abuf.at[k], a_s, a_r)
+    gt = plane(lambda k: tbuf.at[c, g], lambda k: tbuf.at[c, k], t_s, t_r.at[g])
+    gc = column(lambda k: wot_ref, lambda k: zbuf.at[k], c_s, c_r)
+    gq = column(lambda k: rt, lambda k: qbuf.at[k], q_s, q_r)
+    ga.start()
+    pltpu.make_async_copy(wsrc.at[g], abuf.at[g], a_r).start()
     for load in small[:6]:
         load.wait()
     half = tbuf.shape[-1]
@@ -161,26 +193,17 @@
         rank = jnp.max(jnp.where(earlier, same, 0.0), axis=1, keepdims=True)
         table = jnp.where(column_of == k, turned * 2.0 + rank, table)
     rt[:, 0:16] = table
-    for load in small[6:]:
-        load.wait()
-    arrived(wsrc, v_s)
-    pl.semaphore_wait(barrier, 2 * NG - 1 + 2 * NZ - 2)
-
-    def plane(src, dst, send, recv):
-        return Exchange(g, NG, lambda k: device(z, k, c), src, dst, send, recv)
-
-    def column(src, dst, send, recv):
-        return Exchange(z, NZ, lambda k: device(k, g, c), src, dst, send, recv)
-
-    others, above = pl.ds(0, NG - 1), pl.ds(0, NZ - 1)
-
-    ga = plane(lambda k: wsrc.at[k], lambda k: abuf.at[k], a_s, a_r)
-    gt = plane(lambda k: tbuf.at[c, g], lambda k: tbuf.at[c, k], t_s, t_r.at[g])
-    gc = column(lambda k: wot_ref, lambda k: zbuf.at[k], c_s, c_r)
-    gq = column(lambda k: rt, lambda k: qbuf.at[k], q_s, q_r)
-    ga.start()
-    pltpu.make_async_copy(wsrc.at[g], abuf.at[g], a_r).start()
     gq.start()
+    for load in loads:
+        load.start()
+    swap = remote(
+        ed_hbm.at[0, :, pl.ds(pl.multiple_of((1 - c) * 1024, 128), 1024)],
+        ed.at[c],
+        x_s.at[2],
+        x_r.at[2],
+        device(z, g, 1 - c),
+    )
+    swap.start()
     qbuf[pl.ds(z, 1), :, 0:16] = rt[:, 0:16][None]
 
     arrived(abuf, a_r)
@@ -222,6 +245,8 @@
         def _():
             remote(zbuf.at[k], wo.at[g & 7], d_s, d_r, device(z, other, c)).start()
 
+    for load in small[6:]:
+        load.wait()
     arrived(qbuf.at[above], q_r)
     routing = qbuf[...].reshape(NZ * 16, 128)
     slots = 16 * NG
@@ -257,12 +282,10 @@
         block = tbuf.at[half_of, k]
         return remote(block, block, u_s, u_r, device(z, g, 1 - c))
 
-    def t_relay(i):
-        k = (g + i) & (NG - 1)
+    for step in FAR_FIRST[NG][:-1]:
+        k = in_turn(g, NG, step)
         arrived(tbuf.at[c, k], t_r.at[k])
         t_forward(c, k).start()
-
-    each(1, NG, t_relay)
     arrived(tbuf.at[1 - c, others], u_r)
 
     for delta in (0, 1, -1, 3, -3, 4):
@@ -322,17 +345,19 @@
                     column_q * held, axis=0, keepdims=True
                 )[None]
 
-    each(0, 4, read_pair)
-    for hp in range(4):
-        from_state = jnp.where(low_half, fs[2 * hp], pltpu.roll(fs[2 * hp + 1], 64, 1))
-        decay = jnp.where(
-            low_half[0:1], decays[2 * hp : 2 * hp + 1], decays[2 * hp + 1 : 2 * hp + 2]
-        )
-        read = decay * from_state + self_terms[hp]
-        read = read * lax.rsqrt(by_head(read * read) / HEAD + EPS)
-        rbuf[pl.ds(g, 1), hp] = (read * jax.nn.silu(block(3, hp))).astype(BF16)[None]
-    gr = plane(lambda k: rbuf.at[g], lambda k: rbuf.at[g], r_s, r_r)
-    gr.start()
+    for part in range(2):
+        each(2 * part, 2 * part + 2, read_pair)
+        for hp in (2 * part, 2 * part + 1):
+            from_state = jnp.where(low_half, fs[2 * hp], pltpu.roll(fs[2 * hp + 1], 64, 1))
+            decay = jnp.where(
+                low_half[0:1], decays[2 * hp : 2 * hp + 1], decays[2 * hp + 1 : 2 * hp + 2]
+            )
+            read = decay * from_state + self_terms[hp]
+            read = read * lax.rsqrt(by_head(read * read) / HEAD + EPS)
+            rbuf[part, pl.ds(g, 1), hp & 1] = (read * jax.nn.silu(block(3, hp))).astype(BF16)[None]
+        plane(
+            lambda k, part=part: rbuf.at[part, g], lambda k, part=part: rbuf.at[part, g], r_s, r_r
+        ).start()
 
     def update_pair(hp):
         keys = kt[pl.ds(hp, 1)][0]
@@ -364,18 +389,24 @@
         arrived(zbuf, d_s)
 
     arrived(wo, d_r)
-    arrived(rbuf.at[others], r_r)
-    partial = dot(wide_rows(rbuf[...]), wo[...].reshape(128, 512), ((1,), (1,)))
+    arrived(rbuf.at[:, others], r_r)
+    partial = dot(
+        jnp.concatenate([wide_rows(rbuf[0]), wide_rows(rbuf[1])], axis=1),
+        wo[...].reshape(128, 512),
+        ((1,), (1,)),
+    )
     psend[...] = partial.astype(BF16).reshape(psend.shape)
     gp = plane(lambda k: psend.at[k], lambda k: pbuf.at[c, k], p_s.at[0], p_r.at[0])
-    gp.start()
     gp_other = Exchange(
         g, NG, lambda k: device(z, k, 1 - c), lambda k: psend.at[k], lambda k: pbuf.at[c, k],
         p_s.at[1], p_r.at[1],
     )
-    gp_other.start(0)
+    for step in FAR_FIRST[NG]:
+        if step:
+            gp.out(step).start()
+        gp_other.out(step).start()
     pbuf[pl.ds(c, 1), pl.ds(g, 1)] = psend[pl.ds(g, 1)][None]
-    arrived(rbuf.at[others], r_s)
+    arrived(rbuf.at[:, others], r_s)
     arrived(psend.at[others], p_r.at[0])
     arrived(psend, p_r.at[1])
     mixed = (pbuf[0].astype(F32) + pbuf[1].astype(F32)).astype(BF16).astype(F32)
@@ -401,6 +432,8 @@
     share.start()
     for load in loads[4:]:
         load.wait()
+    swap.wait_send()
+    arrived(ed.at[1 - c], x_r.at[2])
     arrived(psend.at[others], p_s.at[0])
     arrived(psend, p_s.at[1])
     for n in range(NCH):
@@ -434,25 +467,16 @@
         gate, up = expert_in(n, 1 - c)
         gates.append(gate)
         ups.append(up)
-    hidden = (jax.nn.silu(sum(gates)) * sum(ups)).astype(BF16)
-
-    def down(n, k):
-        cols_of = pl.ds(pl.multiple_of(k * half + n * PER * 128, 128), PER * 128)
-        out = dot(hidden, ed[0, :, cols_of]).astype(BF16)
-        return [out[:, j * 128 : (j + 1) * 128].reshape(NG, 16, 128) for j in range(PER)]
-
-    def give(n):
-        return remote(dsend.at[n], dbuf.at[n], e_s.at[n], e_r.at[n], device(z, g, 1 - c))
-
-    for n in range(NCH):
-        for j, rows in enumerate(down(n, 1 - c)):
-            dsend[n, :, j] = rows
-        give(n).start()
-    for n in range(NCH):
-        kept = down(n, c)
-        give(n).wait_recv()
+    hid[pl.ds(c, 1)] = (jax.nn.silu(sum(gates)) * sum(ups)).astype(BF16)[None]
+    give = remote(hid.at[c], hid.at[c], x_s.at[3], x_r.at[3], device(z, g, 1 - c))
+    give.start()
+    arrived(hid.at[1 - c], x_r.at[3])
+    hidden = jnp.concatenate([hid[0], hid[1]], axis=1)
+    for n in range(NCH):
+        cols_of = slice(n * PER * 128, (n + 1) * PER * 128)
+        rows_out = dot(hidden, ed[:, :, cols_of].reshape(512, PER * 128)).astype(BF16)
         for j in range(PER):
-            ret[n, :, j] = (kept[j].astype(F32) + dbuf[n, :, j].astype(F32)).astype(BF16)
+            ret[n, :, j] = rows_out[:, j * 128 : (j + 1) * 128].reshape(NG, 16, 128)
         gg = plane(lambda k, n=n: ret.at[n, k], lambda k, n=n: back.at[n, k], g_s, g_r.at[n])
         gg.start()
         back[n, pl.ds(g, 1)] = ret[n, pl.ds(g, 1)]
@@ -461,7 +485,7 @@
     arrived(ysend.at[:, others], y_s)
     for n in range(NCH):
         forward(n).wait_send()
-        give(n).wait_send()
+    give.wait_send()
     share.wait_send()
 
     for n in range(NCH):
@@ -523,7 +547,9 @@
         out_specs=(vmem, anywhere),
         scratch_shapes=[
             pltpu.VMEM(prior_state.shape, F32),
-            *(pltpu.VMEM(array.shape, array.dtype) for array in small + big[1:]),
+            *(pltpu.VMEM(array.shape, array.dtype) for array in small + big[1:3]),
+            pltpu.VMEM((2, 256, 1024), BF16),
+            *(pltpu.VMEM(array.shape, array.dtype) for array in big[4:]),
             blocks,
             pltpu.VMEM((16, 128), F32),
             pltpu.VMEM((16, 128), F32),
@@ -544,7 +570,7 @@
             pltpu.VMEM((8, 16, 128), F32),
             pltpu.VMEM((8, 16, 128), F32),
             pltpu.VMEM((8, 128), F32),
-            pltpu.VMEM((NG, 4, 16, 128), BF16),
+            pltpu.VMEM((2, NG, 2, 16, 128), BF16),
             blocks,
             pltpu.VMEM((2, NG, 16, 128), BF16),
             blocks,
@@ -556,12 +582,11 @@
             pltpu.VMEM((NCH, 2, NG, PER, 16, 128), BF16),
             halves,
             halves,
-            halves,
-            halves,
             columns_of,
             columns_of,
             pltpu.VMEM((8, 16, 128), F32),
             pltpu.VMEM((8, 16, 128), F32),
+            pltpu.VMEM((2, 256, 256), BF16),
             dma((len(small),)),
             dma,
             dma((8,)),
@@ -575,10 +600,9 @@
             dma, chunk_sems,
             dma, chunk_sems,
             chunk_sems, chunk_sems,
-            chunk_sems, chunk_sems,
             dma, chunk_sems,
             dma, chunk_sems,
-            dma((2,)), dma((2,)),
+            dma((4,)), dma((4,)),
         ],
         compiler_params=pltpu.CompilerParams(
             collective_id=0, has_side_effects=True, vmem_limit_bytes=int(59.5 * 2**20)

time: 84.6 us -> 79.3 us (0.937)
  Pallas kernels: 81.3 us -> 75.9 us
    pallas_call x1, Pallas kernels: 81.3 us -> 75.9 us  [on_device(): pl.pallas_call(layer_kernel, out_shape=(pltpu.VMEM((seq, width), BF16), p...]
where the time goes in v5:
time: 79.3 us; the launch traced here: 79.2 us
  Pallas kernels  75.9 us (96%)
  local copies, waits for them, and re-layouts  2.64 us (3%)
    pallas_call x1, Pallas kernels, on_device(): pl.pallas_call(layer_kernel, out_shape=(pltpu.VMEM((seq, width), BF16), p...  75.9 us
    unnamed x2, local copies, waits for them, and re-layouts  2.64 us

profile of v5, /device:TPU:1, one launch (start us, length us, event | category | flops | bytes accessed | tf_op | source)
XLA Modules:
  0.0 79.2 jit_solution(209080846455184060)
XLA Ops:
  0.6 75.9 %layer.1 = (bf16[16,2048]{1,0:T(8,128)(2,1)S(1)}, f32[16,8,64,64]{3,2,1,0:T(8,128)S(1)}) custom-call(bf16[16,2048]{1,0:T(8,128)(2,1)} %tokens_hbm.1, s32[6,16]{1,0:T(8,128)} %bitcast.13, f32[6,16]{1,0:T(8,128)} %bitcast.14, s32[1,16]{1,0:T(1,128)} %bitcast.15, f32[1,128]{1,0:T(1,128)} %constant.2.clone.freq_hbm, f32[1,2048]{1,0:T(1,128)} %bitcast.9, ...), custom_call_target="tpu_custom_call" | custom-call | tf_op jit(solution)/shard_map/layer/pallas_call | solution.py:540
  76.5 0.6 copy.25
  77.2 2.0 %copy.26 = f32[16,8,64,64]{3,2,1,0:T(8,128)} copy(f32[16,8,64,64]{3,2,1,0:T(8,128)S(1)} %get-tuple-element.3) | data formatting | bytes 4194304

commit v6 on v5

--- a/solution.py
+++ b/solution.py
@@ -107,16 +107,16 @@
     wsrc, packed, rt, trig,
     tbuf, abuf, wbuf, zbuf, wo, osend, obuf, qbuf, onehot, comb_hi, comb_lo,
     qt, kt, vsc, fs, decays, rbuf, psend, pbuf, middle, mo, mbuf, shs, shb, ysend, ebuf, ret, back,
-    csend, cbuf, mixs, mixb, hid,
+    csend, cbuf, mixs, mixb,
     i_s, v_s, w_s, a_s, a_r, t_s, t_r, u_s, u_r, b_s, n_s, b_r, c_s, c_r, d_s, d_r, q_s, q_r,
-    o_s, o_r, r_s, r_r, p_s, p_r, m_s, m_r, y_s, y_r, f_s, f_r, g_s, g_r, h_s, h_r, x_s, x_r,
+    o_s, o_r, r_s, r_r, p_s, p_r, m_s, m_r, y_s, y_r, g_s, g_r, h_s, h_r, x_s, x_r,
 ):
     z, g, c = place()
     loads = [
         pltpu.make_async_copy(src, dst, w_s.at[i])
         for i, (src, dst) in enumerate(
             ((state_hbm, state), (sg_hbm, sg), (su_hbm, su), (sd_hbm, sd),
-             (eg_hbm, eg), (eu_hbm, eu), (ed_hbm.at[0, :, pl.ds(pl.multiple_of(c * 1024, 128), 1024)], ed.at[c]))
+             (eg_hbm.at[0], eg.at[c]), (eu_hbm.at[0], eu.at[c]), (ed_hbm.at[0], ed.at[c]))
         )
     ]
     barrier = pltpu.get_barrier_semaphore()
@@ -196,40 +196,39 @@
     gq.start()
     for load in loads:
         load.start()
-    swap = remote(
-        ed_hbm.at[0, :, pl.ds(pl.multiple_of((1 - c) * 1024, 128), 1024)],
-        ed.at[c],
-        x_s.at[2],
-        x_r.at[2],
-        device(z, g, 1 - c),
-    )
-    swap.start()
     qbuf[pl.ds(z, 1), :, 0:16] = rt[:, 0:16][None]
 
     arrived(abuf, a_r)
 
-    def b_copy(delta):
+    def part_of(array, half_of):
+        return array.at[pl.ds(half_of * 8, 8)]
+
+    def b_copy(delta, half_of):
         return remote(
-            abuf, wbuf.at[z], b_s, b_r.at[z], device((z + delta) & (NZ - 1), g, c)
+            part_of(abuf, half_of),
+            part_of(wbuf.at[z], half_of),
+            b_s,
+            b_r.at[z, half_of],
+            device((z + delta) & (NZ - 1), g, c),
         )
 
-    for delta in (2, -2, 1, -1):
-        b_copy(delta).start()
-    pltpu.make_async_copy(abuf, wbuf.at[z], b_r.at[z]).start()
+    for delta, half_of in ((2, 0), (-2, 0), (2, 1), (-2, 1), (1, 0), (-1, 0), (1, 1), (-1, 1)):
+        b_copy(delta, half_of).start()
+    for half_of in range(2):
+        pltpu.make_async_copy(
+            part_of(abuf, half_of), part_of(wbuf.at[z], half_of), b_r.at[z, half_of]
+        ).start()
     gt.start()
 
-    def b_wait(delta):
+    def b_wait(delta, half_of):
         source = (z + delta) & (NZ - 1)
-        pltpu.make_async_copy(abuf, wbuf.at[source], b_r.at[source]).wait()
-
-    def onward(delta, to):
+        arrived(part_of(wbuf.at[source], half_of), b_r.at[source, half_of])
+
+    def onward(delta, to, half_of):
         source = (z + delta) & (NZ - 1)
+        block = part_of(wbuf.at[source], half_of)
         return remote(
-            wbuf.at[source],
-            wbuf.at[source],
-            n_s,
-            b_r.at[source],
-            device((z + to) & (NZ - 1), g, c),
+            block, block, n_s, b_r.at[source, half_of], device((z + to) & (NZ - 1), g, c)
         )
 
     to_half = g >> 3
@@ -272,11 +271,12 @@
     trig[1] = jnp.where(first, -sines, sines)
     heads = lax.broadcasted_iota(jnp.int32, (8, 128), 0) + c * 8
     decays[...] = 1.0 - jnp.exp2(-5.0 - 7.0 * heads.astype(F32) / (HEADS - 1))
-    b_wait(-2)
-    onward(-2, 2).start()
-    onward(-2, 1).start()
-    b_wait(2)
-    onward(2, -1).start()
+    for half_of in range(2):
+        b_wait(-2, half_of)
+        onward(-2, 2, half_of).start()
+        onward(-2, 1, half_of).start()
+        b_wait(2, half_of)
+        onward(2, -1, half_of).start()
 
     def t_forward(half_of, k):
         block = tbuf.at[half_of, k]
@@ -289,7 +289,8 @@
     arrived(tbuf.at[1 - c, others], u_r)
 
     for delta in (0, 1, -1, 3, -3, 4):
-        b_wait(delta)
+        b_wait(delta, 0)
+        b_wait(delta, 1)
     rows = NG * tbuf.shape[2]
     mine = dot(tbuf[0].reshape(rows, half), wbuf[0:4].reshape(half, 128)) + dot(
         tbuf[1].reshape(rows, half), wbuf[4:8].reshape(half, 128)
@@ -297,6 +298,12 @@
     osend[...] = mine.astype(BF16).reshape(osend.shape)
     go = plane(lambda k: osend.at[k], lambda k: obuf.at[k], o_s, o_r)
     go.start()
+    swaps = [
+        remote(src.at[0], dst.at[c], x_s.at[2 + i], x_r.at[2 + i], device(z, g, 1 - c))
+        for i, (src, dst) in enumerate(((eg_hbm, eg), (eu_hbm, eu), (ed_hbm, ed)))
+    ]
+    for swap in swaps:
+        swap.start()
     gc = column(lambda k: wot_ref, lambda k: zbuf.at[z], c_s, c_r)
     gc.start()
     pltpu.make_async_copy(wot_ref, zbuf.at[z], c_r).start()
@@ -432,8 +439,10 @@
     share.start()
     for load in loads[4:]:
         load.wait()
-    swap.wait_send()
-    arrived(ed.at[1 - c], x_r.at[2])
+    for i, (swap, dst) in enumerate(zip(swaps, (eg, eu, ed))):
+        swap.wait_send()
+        arrived(dst.at[1 - c], x_r.at[2 + i])
+    home = g & 1
     arrived(psend.at[others], p_s.at[0])
     arrived(psend, p_s.at[1])
     for n in range(NCH):
@@ -441,55 +450,81 @@
         sorted_rows = dot(onehot[...], wide_rows(mbuf[n])).astype(BF16)
         for k in range(PER):
             ysend[n, :, k] = sorted_rows[:, k * 128 : (k + 1) * 128].reshape(NG, 16, 128)
-        gy = plane(lambda k, n=n: ysend.at[n, k], lambda k, n=n: ebuf.at[n, c, k], y_s, y_r.at[n])
-        gy.start()
-        ebuf[n, pl.ds(c, 1), pl.ds(g, 1)] = ysend[n, pl.ds(g, 1)][None]
+
+        def to_expert(k, n=n):
+            return remote(
+                ysend.at[n, k], ebuf.at[n, c, g >> 1], y_s, y_r.at[n], device(z, k, home)
+            )
+
+        for step in FAR_FIRST[NG][:-1]:
+            to_expert(in_turn(g, NG, step)).start()
+
+        @pl.when(home == c)
+        def _(n=n):
+            pltpu.make_async_copy(ysend.at[n, g], ebuf.at[n, c, g >> 1], y_r.at[n]).start()
+
+        @pl.when(home != c)
+        def _(to_expert=to_expert):
+            to_expert(g).start()
+
     arrived(mbuf.at[:, above], m_s)
 
-    def forward(n):
-        rows = ebuf.at[n, c]
-        return remote(rows, rows, f_s.at[n], f_r.at[n], device(z, g, 1 - c))
-
-    def expert_in(n, k):
-        blocks = wide_rows(ebuf[n, pl.ds(k, 1)][0])
-        rows_of = pl.ds(pl.multiple_of(k * half + n * PER * 128, 128), PER * 128)
-        return dot(blocks, eg[0, rows_of]), dot(blocks, eu[0, rows_of])
-
-    gates, ups = [], []
+    gates, ups = [0.0, 0.0], [0.0, 0.0]
     for n in range(NCH):
-        arrived(ebuf.at[n, c, others], y_r.at[n])
-        forward(n).start()
-        gate, up = expert_in(n, c)
-        gates.append(gate)
-        ups.append(up)
+        arrived(ebuf.at[n], y_r.at[n])
+        for h in range(2):
+            blocks = wide_rows(ebuf[n, h])
+            rows_of = slice(h * half + n * PER * 128, h * half + (n + 1) * PER * 128)
+            for f in range(2):
+                gates[f] += dot(blocks, eg[f, rows_of])
+                ups[f] += dot(blocks, eu[f, rows_of])
+    hidden = jnp.concatenate(
+        [(jax.nn.silu(gates[f]) * ups[f]).astype(BF16) for f in range(2)], axis=1
+    )
+    turns = [(dy, dd) for dy in (2, 1, 3, 0) for dd in (1, 0)]
+    odd = (g ^ c) & 1
     for n in range(NCH):
-        arrived(ebuf.at[n, 1 - c], f_r.at[n])
-        gate, up = expert_in(n, 1 - c)
-        gates.append(gate)
-        ups.append(up)
-    hid[pl.ds(c, 1)] = (jax.nn.silu(sum(gates)) * sum(ups)).astype(BF16)[None]
-    give = remote(hid.at[c], hid.at[c], x_s.at[3], x_r.at[3], device(z, g, 1 - c))
-    give.start()
-    arrived(hid.at[1 - c], x_r.at[3])
-    hidden = jnp.concatenate([hid[0], hid[1]], axis=1)
-    for n in range(NCH):
-        cols_of = slice(n * PER * 128, (n + 1) * PER * 128)
-        rows_out = dot(hidden, ed[:, :, cols_of].reshape(512, PER * 128)).astype(BF16)
-        for j in range(PER):
-            ret[n, :, j] = rows_out[:, j * 128 : (j + 1) * 128].reshape(NG, 16, 128)
-        gg = plane(lambda k, n=n: ret.at[n, k], lambda k, n=n: back.at[n, k], g_s, g_r.at[n])
-        gg.start()
-        back[n, pl.ds(g, 1)] = ret[n, pl.ds(g, 1)]
+        for h in range(2):
+            cols_of = slice(h * half + n * PER * 128, h * half + (n + 1) * PER * 128)
+            rows_out = dot(hidden, ed[:, :, cols_of].reshape(512, PER * 128)).astype(BF16)
+            for j in range(PER):
+                ret[n, h, :, j] = rows_out[:, j * 128 : (j + 1) * 128].reshape(8, 16, 128)
+        for dy, dd in turns:
+            k = ((g + 4 * dy) & 12) + ((g + odd + 2 * dd) & 3)
+            for h in range(2):
+
+                def give_back(k=k, n=n, h=h):
+                    return remote(
+                        ret.at[n, h, k >> 1], back.at[n, g], g_s, g_r.at[n], device(z, k, h)
+                    )
+
+                if (dy, dd) != (0, 0):
+                    give_back().start()
+                    continue
+                here = jnp.logical_and(k == g, c == h)
+
+                @pl.when(here)
+                def _(n=n, h=h):
+                    pltpu.make_async_copy(
+                        ret.at[n, h, g >> 1], back.at[n, g], g_r.at[n]
+                    ).start()
+
+                @pl.when(jnp.logical_not(here))
+                def _(give_back=give_back):
+                    give_back().start()
+
     share.wait_recv()
     shared_out = (shs[pl.ds(c, 1)][0].astype(F32) + shb[...].astype(F32)).astype(BF16).astype(F32)
     arrived(ysend.at[:, others], y_s)
+
+    @pl.when(home != c)
+    def _():
+        arrived(ysend.at[:, 0], y_s)
+
+    share.wait_send()
+
     for n in range(NCH):
-        forward(n).wait_send()
-    give.wait_send()
-    share.wait_send()
-
-    for n in range(NCH):
-        arrived(back.at[n, others], g_r.at[n])
+        arrived(back.at[n], g_r.at[n])
         answers = wide_rows(back[n])
         sums = (dot(comb_hi[...], answers) + dot(comb_lo[...], answers)).astype(BF16)
         for k in range(PER):
@@ -497,7 +532,12 @@
         gh = column(lambda k, n=n: csend.at[n, k], lambda k, n=n: cbuf.at[n, k], h_s, h_r.at[n])
         gh.start()
         cbuf[n, pl.ds(z, 1)] = csend[n, pl.ds(z, 1)]
-    arrived(ret.at[:, others], g_s)
+    arrived(back.at[:, others], g_s)
+
+    @pl.when(home != c)
+    def _():
+        arrived(back.at[:, 0], g_s)
+
     for n in range(NCH):
         arrived(cbuf.at[n, above], h_r.at[n])
         part = slice(n * PER, (n + 1) * PER)
@@ -547,8 +587,8 @@
         out_specs=(vmem, anywhere),
         scratch_shapes=[
             pltpu.VMEM(prior_state.shape, F32),
-            *(pltpu.VMEM(array.shape, array.dtype) for array in small + big[1:3]),
-            pltpu.VMEM((2, 256, 1024), BF16),
+            *(pltpu.VMEM(array.shape, array.dtype) for array in small),
+            *(pltpu.VMEM((2, *array.shape[1:]), BF16) for array in big[1:4]),
             *(pltpu.VMEM(array.shape, array.dtype) for array in big[4:]),
             blocks,
             pltpu.VMEM((16, 128), F32),
@@ -579,30 +619,28 @@
             pltpu.VMEM((2, 8, 16, 128), BF16),
             pltpu.VMEM((8, 16, 128), BF16),
             halves,
-            pltpu.VMEM((NCH, 2, NG, PER, 16, 128), BF16),
-            halves,
+            pltpu.VMEM((NCH, 2, 8, PER, 16, 128), BF16),
+            pltpu.VMEM((NCH, 2, 8, PER, 16, 128), BF16),
             halves,
             columns_of,
             columns_of,
             pltpu.VMEM((8, 16, 128), F32),
             pltpu.VMEM((8, 16, 128), F32),
-            pltpu.VMEM((2, 256, 256), BF16),
             dma((len(small),)),
             dma,
             dma((8,)),
             dma, dma,
             dma, dma((NG,)),
             dma, dma,
-            dma, dma, dma((NZ,)),
+            dma, dma, dma((NZ, 2)),
             dma, dma, dma, dma, dma, dma,
             dma, dma, dma, dma,
             dma((2,)), dma((2,)),
             dma, chunk_sems,
             dma, chunk_sems,
-            chunk_sems, chunk_sems,
             dma, chunk_sems,
             dma, chunk_sems,
-            dma((4,)), dma((4,)),
+            dma((5,)), dma((5,)),
         ],
         compiler_params=pltpu.CompilerParams(
             collective_id=0, has_side_effects=True, vmem_limit_bytes=int(59.5 * 2**20)

time: 79.3 us -> 77.6 us (0.979)
  Pallas kernels: 75.9 us -> 74.2 us
    pallas_call x1, Pallas kernels: 75.9 us -> 74.2 us  [on_device(): pl.pallas_call(layer_kernel, out_shape=(pltpu.VMEM((seq, width), BF16), p...]
where the time goes in v6:
time: 77.6 us; the launch traced here: 77.5 us
  Pallas kernels  74.2 us (96%)
  local copies, waits for them, and re-layouts  2.64 us (3%)
    pallas_call x1, Pallas kernels, on_device(): pl.pallas_call(layer_kernel, out_shape=(pltpu.VMEM((seq, width), BF16), p...  74.2 us
    unnamed x2, local copies, waits for them, and re-layouts  2.64 us

profile of v6, /device:TPU:1, one launch (start us, length us, event | category | flops | bytes accessed | tf_op | source)
XLA Modules:
  0.0 77.5 jit_solution(1168449940313573485)
XLA Ops:
  0.6 74.2 %layer.1 = (bf16[16,2048]{1,0:T(8,128)(2,1)S(1)}, f32[16,8,64,64]{3,2,1,0:T(8,128)S(1)}) custom-call(bf16[16,2048]{1,0:T(8,128)(2,1)} %tokens_hbm.1, s32[6,16]{1,0:T(8,128)} %bitcast.13, f32[6,16]{1,0:T(8,128)} %bitcast.14, s32[1,16]{1,0:T(1,128)} %bitcast.15, f32[1,128]{1,0:T(1,128)} %constant.2.clone.freq_hbm, f32[1,2048]{1,0:T(1,128)} %bitcast.9, ...), custom_call_target="tpu_custom_call" | custom-call | tf_op jit(solution)/shard_map/layer/pallas_call | solution.py:580
  74.8 0.6 copy.25
  75.5 2.0 %copy.26 = f32[16,8,64,64]{3,2,1,0:T(8,128)} copy(f32[16,8,64,64]{3,2,1,0:T(8,128)S(1)} %get-tuple-element.3) | data formatting | bytes 4194304

commit v7 on v6

--- a/solution.py
+++ b/solution.py
@@ -19,7 +19,7 @@
 FAR_FIRST = {
     NZ: sorted(range(NZ), key=lambda step: -min(step, NZ - step)),
     NG: sorted(
-        range(NG), key=lambda step: -min(step // 4, 4 - step // 4) - min(step % 4, 4 - step % 4)
+        range(NG), key=lambda step: (-min(step // 4, 4 - step // 4) - min(step % 4, 4 - step % 4), (step * 7) % 16)
     ),
 }
 BF16 = jnp.bfloat16
@@ -298,12 +298,6 @@
     osend[...] = mine.astype(BF16).reshape(osend.shape)
     go = plane(lambda k: osend.at[k], lambda k: obuf.at[k], o_s, o_r)
     go.start()
-    swaps = [
-        remote(src.at[0], dst.at[c], x_s.at[2 + i], x_r.at[2 + i], device(z, g, 1 - c))
-        for i, (src, dst) in enumerate(((eg_hbm, eg), (eu_hbm, eu), (ed_hbm, ed)))
-    ]
-    for swap in swaps:
-        swap.start()
     gc = column(lambda k: wot_ref, lambda k: zbuf.at[z], c_s, c_r)
     gc.start()
     pltpu.make_async_copy(wot_ref, zbuf.at[z], c_r).start()
@@ -318,6 +312,12 @@
     arrived(obuf.at[others], o_r)
     arrived(zbuf, c_r)
     each(0, NZ, d_start)
+    swaps = [
+        remote(src.at[0], dst.at[c], x_s.at[2 + i], x_r.at[2 + i], device(z, g, 1 - c))
+        for i, (src, dst) in enumerate(((eg_hbm, eg), (eu_hbm, eu), (ed_hbm, ed)))
+    ]
+    for swap in swaps:
+        swap.start()
     low_half = lax.broadcasted_iota(jnp.int32, (16, 128), 1) < 64
     def rotate(v):
         other = jnp.where(first, pltpu.roll(v, 96, 1), pltpu.roll(v, 32, 1))

time: 77.6 us -> 77.6 us (level)
  no operation moved by 1% of the time
where the time goes in v7:
time: 77.6 us; the launch traced here: 77.4 us
  Pallas kernels  74.2 us (96%)
  local copies, waits for them, and re-layouts  2.64 us (3%)
    pallas_call x1, Pallas kernels, on_device(): pl.pallas_call(layer_kernel, out_shape=(pltpu.VMEM((seq, width), BF16), p...  74.2 us
    unnamed x2, local copies, waits for them, and re-layouts  2.64 us

profile of v7, /device:TPU:1, one launch (start us, length us, event | category | flops | bytes accessed | tf_op | source)
XLA Modules:
  0.0 77.4 jit_solution(8098871573220134181)
XLA Ops:
  0.6 74.2 %layer.1 = (bf16[16,2048]{1,0:T(8,128)(2,1)S(1)}, f32[16,8,64,64]{3,2,1,0:T(8,128)S(1)}) custom-call(bf16[16,2048]{1,0:T(8,128)(2,1)} %tokens_hbm.1, s32[6,16]{1,0:T(8,128)} %bitcast.13, f32[6,16]{1,0:T(8,128)} %bitcast.14, s32[1,16]{1,0:T(1,128)} %bitcast.15, f32[1,128]{1,0:T(1,128)} %constant.2.clone.freq_hbm, f32[1,2048]{1,0:T(1,128)} %bitcast.9, ...), custom_call_target="tpu_custom_call" | custom-call | tf_op jit(solution)/shard_map/layer/pallas_call | solution.py:580
  74.8 0.6 copy.25
  75.4 2.0 %copy.26 = f32[16,8,64,64]{3,2,1,0:T(8,128)} copy(f32[16,8,64,64]{3,2,1,0:T(8,128)S(1)} %get-tuple-element.3) | data formatting | bytes 4194304
